TPU v7x, 128 devices: a whole 4x4x4 slice. The times are simulated.
128 devices in a mesh: sp: 32 (over z, y, core), tp: 4 (over x).
Axes of the slice: x: 4, y: 4, z: 4, core: 2. Of those that a mesh axis runs over, the one named last changes fastest.
Arguments:
- tokens: bfloat16 [8192, 4096], P(('sp', 'tp')), may hold values from -700 to 700
- down_query: bfloat16 [4096, 1024], replicated, may hold values from -0.09375 to 0.09375
- down_latent: bfloat16 [4096, 512], replicated, may hold values from -0.09375 to 0.09375
- down_rotary: bfloat16 [4096, 64], replicated, may hold values from -0.09375 to 0.09375
- query_gain: float32 [1024], replicated, may hold values from 0.1 to 1.9
- latent_gain: float32 [512], replicated, may hold values from 0.1 to 1.9
- up_query: bfloat16 [1024, 2048], P(None, 'tp'), may hold values from -0.1875 to 0.1875
- up_query_rotary: bfloat16 [1024, 1024], P(None, 'tp'), may hold values from -0.1875 to 0.1875
- up_key: bfloat16 [512, 2048], P(None, 'tp'), may hold values from -0.25 to 0.25
- up_value: bfloat16 [512, 2048], P(None, 'tp'), may hold values from -0.25 to 0.25
- out_weight: bfloat16 [2048, 4096], P('tp'), may hold values from -0.39648438 to 0.39648438
Outputs:
- mixed: bfloat16 [8192, 4096], P(('sp', 'tp'))
All inputs are finite; a program needn't handle non-finite values.
Results may differ from a plain program's by a relative error of at most 0.03.
Values may be sent and summed in bfloat16 or wider, within the bound.
A program may use at most 192 MiB of HBM per device.

v0:
```python
import functools

import jax
import jax.numpy as jnp
import numpy as np
from jax import lax
from jax.experimental import pallas as pl
from jax.experimental.pallas import tpu as pltpu
from jax.sharding import PartitionSpec as P

NOPE = 128
ROPE = 64
VDIM = 128
LANES = 128

rope_base = 500000.0
norm_eps = 1e-06
masked_score = -1e30
log2e = 1.4426950408889634

MESH = pl.DeviceIdType.MESH
F32 = jnp.float32
BF16 = jnp.bfloat16


def dot(a, b):
    return jnp.dot(a, b, preferred_element_type=F32)


def dot_nt(a, b):
    return lax.dot_general(a, b, (((1,), (1,)), ((), ())), preferred_element_type=F32)


def turn(v, cosine, sine):
    lane = lax.broadcasted_iota(jnp.int32, v.shape, 1)
    other = jnp.where(lane % ROPE < ROPE // 2, pltpu.roll(v, LANES - ROPE // 2, 1), pltpu.roll(v, ROPE // 2, 1))
    return v * cosine + other * sine


def normed(v, gain):
    return v * lax.rsqrt(jnp.mean(v * v, axis=-1, keepdims=True) + norm_eps) * gain


def kernel(
    S,
    T,
    chunks,
    pieces,
    tokens_hbm,
    dq_hbm,
    dl_hbm,
    dr_hbm,
    qg_ref,
    lg_ref,
    uq_hbm,
    ur_hbm,
    uk_hbm,
    uv_hbm,
    ow_hbm,
    base_cos,
    base_sin,
    row_cos,
    row_sin,
    out_ref,
    tokens,
    dq,
    dl,
    dr,
    uq,
    ur,
    uk,
    uv,
    ow,
    kv,
    ql,
    qh,
    acc,
    best,
    att,
    pair_out,
    pair_in,
    kept,
    cross_out,
    cross_in,
    uvt,
    first_keys,
    first_values,
    cos_ref,
    sin_ref,
    load_sem,
    kv_send,
    kv_recv,
    q_send,
    q_recv,
    pair_send,
    pair_recv,
    cross_send,
    cross_recv,
):
    O = S // 2
    rows = tokens.shape[0]
    span = rows * T
    depth = tokens.shape[1]
    heads = qh.shape[0]
    rank = dl.shape[1]
    sp = lax.axis_index("sp")
    tp = lax.axis_index("tp")
    o, i = sp // 2, sp % 2
    g, c = tp // 2, tp % 2

    def dev(o_, i_, g_, c_):
        return {"sp": o_ * 2 + i_, "tp": g_ * 2 + c_}

    across = dev(o, i, 1 - g, c)
    beside = dev(o, 1 - i, g, c)
    mate = dev(o, i, g, 1 - c)

    step = depth // chunks
    loads = []

    def load(src, dst):
        copy = pltpu.make_async_copy(src, dst, load_sem.at[len(loads)])
        loads.append(copy)
        copy.start()
        return copy

    tok_load = load(tokens_hbm, tokens)
    dl_loads = [load(dl_hbm.at[pl.ds(k * step, step)], dl.at[pl.ds(k * step, step)]) for k in range(chunks)]
    dr_load = load(dr_hbm, dr)
    dq_loads = [load(dq_hbm.at[pl.ds(k * step, step)], dq.at[pl.ds(k * step, step)]) for k in range(chunks)]
    up_loads = [load(uq_hbm, uq), load(ur_hbm, ur), load(uk_hbm, uk), load(uv_hbm, uv)]
    ow_load = load(ow_hbm, ow)

    barrier = pltpu.get_barrier_semaphore()
    for d in range(1, O):
        pl.semaphore_signal(barrier, inc=1, device_id=dev((o + d) % O, i, g, c), device_id_type=MESH)
    for target in (across, beside, mate):
        pl.semaphore_signal(barrier, inc=1, device_id=target, device_id_type=MESH)

    def block(o_, i_, g_, c_):
        return (o_ * 2 + i_) * T + g_ * 2 + c_

    def block_rows(b):
        return pl.ds(pl.multiple_of(b * rows, rows), rows)

    def kv_copy(b, target, index):
        part = kv.at[block_rows(b)]
        return pltpu.make_async_remote_copy(
            src_ref=part,
            dst_ref=part,
            send_sem=kv_send.at[index],
            recv_sem=kv_recv.at[b],
            device_id=target,
            device_id_type=MESH,
        )

    def kv_wait(b):
        kv_copy(b, mate, 0).wait_recv()

    start_cos, start_sin = base_cos[pl.ds(sp, 1), :], base_sin[pl.ds(sp, 1), :]
    sign = jnp.where(lax.broadcasted_iota(jnp.int32, (1, LANES), 1) % ROPE < ROPE // 2, -1.0, 1.0)
    cos_ref[...] = start_cos * row_cos[...] - start_sin * row_sin[...]
    sin_ref[...] = (start_sin * row_cos[...] + start_cos * row_sin[...]) * sign

    tok_load.wait()
    latent = jnp.zeros((rows, rank), F32)
    for k in range(chunks):
        dl_loads[k].wait()
        latent += dot(tokens[:, k * step : (k + 1) * step], dl[k * step : (k + 1) * step, :])
    dr_load.wait()
    turned = dot_nt(tokens[...], dr[...])
    turned = jnp.concatenate([turned, jnp.zeros((rows, LANES - ROPE), F32)], axis=1)
    own_rows = pl.ds(pl.multiple_of(tp * rows, rows), rows)
    mine = block_rows(block(o, i, g, c))
    kv[mine, :rank] = normed(latent, lg_ref[...]).astype(BF16)
    kv[mine, rank:] = turn(turned, cos_ref[own_rows, :], sin_ref[own_rows, :]).astype(BF16)

    pl.semaphore_wait(barrier, O - 1 + 3)

    def up_copy(d):
        return kv_copy(block(o, i, g, c), dev((o + d) % O, i, g, c), d)

    def relay_near(d, act):
        b = block(o - d, i, g, c)
        act(kv_copy(b, across, O + d))

        @pl.when((i == 0) | (d > 0))
        def _():
            act(kv_copy(b, beside, 2 * O + 2 * d))

        act(kv_copy(b, mate, 4 * O + 4 * d))

    def relay_far(d, act):
        b = block(o - d, i, 1 - g, c)

        @pl.when(((i == 0) | (d > 0)) & (d < O - 1))
        def _():
            act(kv_copy(b, beside, 2 * O + 2 * d + 1))

        act(kv_copy(b, mate, 4 * O + 4 * d + 1))

    def relay_beside(d, act):
        b = block(o - d, 1 - i, g, c)

        @pl.when(d == O - 1)
        def _():
            act(kv_copy(b, across, 2 * O + 2 * d + 1))

        act(kv_copy(b, mate, 4 * O + 4 * d + 2))

    def relay_corner(d, act):
        act(kv_copy(block(o - d, 1 - i, 1 - g, c), mate, 4 * O + 4 * d + 3))

    def start(copy):
        copy.start()

    def sent(copy):
        copy.wait_send()

    def near(d):
        kv_wait(block(o - d, i, g, c))
        relay_near(d, start)

    def far(d):
        kv_wait(block(o - d, i, 1 - g, c))
        relay_far(d, start)

    def beside_in(d):
        kv_wait(block(o - d, 1 - i, g, c))
        relay_beside(d, start)

    def corner_in(d):
        kv_wait(block(o - d, 1 - i, 1 - g, c))
        relay_corner(d, start)

    def each(first, body):
        def run(d, carry):
            body(d)
            return carry

        lax.fori_loop(first, o + 1, run, 0)

    for d in range(1, O):

        @pl.when(o + d < O)
        def _(d=d):
            up_copy(d).start()

    relay_near(0, start)

    query = jnp.zeros((rows, dq.shape[1]), F32)
    for k in range(chunks):
        dq_loads[k].wait()
        query += dot(tokens[:, k * step : (k + 1) * step], dq[k * step : (k + 1) * step, :])
    ql[own_rows, :] = normed(query, qg_ref[...]).astype(BF16)

    def q_copy(t, target, index):
        part = ql.at[block_rows(t)]
        return pltpu.make_async_remote_copy(
            src_ref=part,
            dst_ref=part,
            send_sem=q_send.at[index],
            recv_sem=q_recv.at[t],
            device_id=target,
            device_id_type=MESH,
        )

    other = (1 - g) * 2 + c
    q_copies = [q_copy(tp, across, 0), q_copy(tp, mate, 1), q_copy(other, mate, 2)]
    q_copies[0].start()
    q_copies[1].start()

    def kv_heads(s):
        part = pl.ds(pl.multiple_of(s * span, span), span)
        lat = kv[part, :rank]
        return dot(lat, uk[...]).astype(BF16), dot_nt(uvt[...], lat).astype(BF16)

    up_loads[2].wait()
    up_loads[3].wait()
    uvt[...] = uv[...].T
    far(0)
    pl.when(o >= 1)(lambda: near(1))
    kv_wait(block(o, i, g, 1 - c))
    kv_wait(block(o, i, 1 - g, 1 - c))
    first_keys[...], first_values[...] = kv_heads(sp)
    each(2, near)

    q_copy(other, mate, 2).wait_recv()
    q_copies[2].start()

    @pl.when(i == 1)
    def _():
        beside_in(0)
        corner_in(0)

    q_copy(g * 2 + 1 - c, mate, 0).wait_recv()
    q_copy((1 - g) * 2 + 1 - c, mate, 0).wait_recv()

    pl.when(o >= 1)(lambda: far(1))
    for copy in up_loads[:2]:
        copy.wait()
    scale = (NOPE + ROPE) ** (-0.5) * log2e
    plain = (dot(ql[...], uq[...]) * scale).astype(BF16)
    turning = dot(ql[...], ur[...]) * scale
    low = lax.broadcasted_iota(jnp.int32, (span, LANES), 1) < ROPE
    for pair in range(heads // 2):
        both = turn(turning[:, pair * LANES : (pair + 1) * LANES], cos_ref[...], sin_ref[...])
        qh[2 * pair, :, NOPE:] = jnp.where(low, both, 0.0).astype(BF16)
        qh[2 * pair + 1, :, NOPE:] = jnp.where(low, pltpu.roll(both, ROPE, 1), 0.0).astype(BF16)
    for h in range(heads):
        qh[h, :, :NOPE] = plain[:, h * NOPE : (h + 1) * NOPE]
        best[h] = jnp.full(best.shape[1:], masked_score, F32)
        acc[h] = jnp.zeros(acc.shape[1:], F32)

    def attend(s, masked=False):
        rot = kv[pl.ds(pl.multiple_of(s * span, span), span), rank:]
        keys, values = (first_keys[...], first_values[...]) if masked else kv_heads(s)
        ones = jnp.ones((acc.shape[1] - VDIM, span), BF16)
        if masked:
            k_pos = lax.broadcasted_iota(jnp.int32, (span, span), 0)
            q_pos = lax.broadcasted_iota(jnp.int32, (span, span), 1)
            allowed = k_pos <= q_pos

        def score(h):
            key = jnp.concatenate([keys[:, h * NOPE : (h + 1) * NOPE], rot], axis=1)
            return dot_nt(key, qh[h])

        ahead = score(0)
        for h in range(heads):
            scores = ahead
            if h + 1 < heads:
                ahead = score(h + 1)
            value = jnp.concatenate([values[h * VDIM : (h + 1) * VDIM], ones], axis=0)
            if masked:
                scores = jnp.where(allowed, scores, masked_score)
            old = best[h][:1]
            new = jnp.maximum(old, jnp.max(scores, axis=0, keepdims=True))
            weights = jnp.exp2(scores - new).astype(BF16)
            acc[h] = acc[h] * jnp.exp2(old - new) + dot(value, weights)
            best[h] = jnp.broadcast_to(new, best.shape[1:])

    def next_to(d):
        kv_wait(block(o - d, 1 - i, g, 1 - c))
        kv_wait(block(o - d, 1 - i, 1 - g, 1 - c))
        attend((o - d) * 2 + 1 - i)

    def column(d):
        pl.when(d + 3 <= o)(lambda: far(d + 3))
        kv_wait(block(o - d, i, g, 1 - c))
        kv_wait(block(o - d, i, 1 - g, 1 - c))
        attend((o - d) * 2 + i)
        corner_in(d)

    pl.when(o >= 2)(lambda: far(2))
    attend(sp, masked=True)
    pl.when(o >= 3)(lambda: far(3))
    each(1, beside_in)
    pl.when(i == 1)(lambda: next_to(0))
    each(1, column)
    each(1, next_to)

    for h in range(heads):
        whole = acc[h]
        att[:, h * VDIM : (h + 1) * VDIM] = (whole[:VDIM] / whole[VDIM : VDIM + 1]).T.astype(BF16)

    ow_load.wait()
    width = ow.shape[1] // pieces
    lag = min(3, pieces)

    def pair_copy(phase, j):
        return pltpu.make_async_remote_copy(
            src_ref=pair_out.at[phase, j],
            dst_ref=pair_in.at[phase, j],
            send_sem=pair_send.at[phase * pieces + j],
            recv_sem=pair_recv.at[phase * pieces + j],
            device_id=mate,
            device_id_type=MESH,
        )

    def cross_copy(j):
        return pltpu.make_async_remote_copy(
            src_ref=cross_out.at[j],
            dst_ref=cross_in.at[j],
            send_sem=cross_send.at[j],
            recv_sem=cross_recv.at[j],
            device_id=across,
            device_id_type=MESH,
        )

    def project(phase, group, j):
        top = att[block_rows(group * 2 + 1 - c), :]
        low_part = att[block_rows(group * 2 + c), :]
        part = dot(jnp.concatenate([top, low_part], axis=0), ow[:, j * width : (j + 1) * width])
        pair_out[phase, j] = part[:rows].astype(BF16)
        kept[phase, j] = part[rows:]
        pair_copy(phase, j).start()

    def cross(j):
        pair_copy(0, j).wait_recv()
        cross_out[j] = (kept[0, j] + pair_in[0, j].astype(F32)).astype(BF16)
        cross_copy(j).start()

    for j in range(pieces):
        project(0, 1 - g, j)
        if j >= lag:
            cross(j - lag)
    for j in range(pieces - lag, pieces):
        cross(j)
    for j in range(pieces):
        project(1, g, j)
    for j in range(pieces):
        pair_copy(1, j).wait_recv()
        cross_copy(j).wait_recv()
        total = kept[1, j] + pair_in[1, j].astype(F32) + cross_in[j].astype(F32)
        out_ref[:, j * width : (j + 1) * width] = total

    for d in range(1, O):

        @pl.when(o + d < O)
        def _(d=d):
            up_copy(d).wait_send()

    def drain(d, carry):
        relay_near(d, sent)
        relay_far(d, sent)

        @pl.when((i == 1) | (d > 0))
        def _():
            relay_beside(d, sent)
            relay_corner(d, sent)

        return carry

    lax.fori_loop(0, o + 1, drain, 0)
    for copy in q_copies:
        copy.wait_send()
    for j in range(pieces):
        pair_copy(0, j).wait_send()
        pair_copy(1, j).wait_send()
        cross_copy(j).wait_send()


def solution(mesh):
    S, T = mesh.shape["sp"], mesh.shape["tp"]
    assert S % 2 == 0 and T == 4

    def local(tokens, dq, dl, dr, qg, lg, uq, ur, uk, uv, ow):
        rows, depth = tokens.shape
        span = rows * T
        heads = uk.shape[1] // NOPE
        width = ow.shape[1]
        rank = dl.shape[1]
        chunks, pieces = 4, 8
        inverse = np.float32(rope_base) ** (-np.arange(0, ROPE, 2, dtype=np.float32) / np.float32(ROPE))
        inverse = np.tile(inverse.astype(np.float64), LANES // (ROPE // 2))
        starts = np.arange(S)[:, None] * span * inverse
        steps = np.arange(span)[:, None] * inverse
        tables = [jnp.asarray(f(a), F32) for a in (starts, steps) for f in (np.cos, np.sin)]
        O = S // 2
        hbm = pl.BlockSpec(memory_space=pl.ANY)
        vmem = pl.BlockSpec(memory_space=pltpu.VMEM)
        dma = lambda n: pltpu.SemaphoreType.DMA((n,))
        like = lambda a: pltpu.VMEM(a.shape, a.dtype)
        total = pl.pallas_call(
            functools.partial(kernel, S, T, chunks, pieces),
            out_shape=jax.ShapeDtypeStruct((rows, width), F32),
            in_specs=[hbm, hbm, hbm, hbm, vmem, vmem, hbm, hbm, hbm, hbm, hbm, vmem, vmem, vmem, vmem],
            out_specs=vmem,
            scratch_shapes=[
                like(tokens),
                like(dq),
                like(dl),
                pltpu.VMEM(dr.shape[::-1], dr.dtype),
                like(uq),
                like(ur),
                like(uk),
                like(uv),
                like(ow),
                pltpu.VMEM((S * span, rank + LANES), BF16),
                pltpu.VMEM((span, dq.shape[1]), BF16),
                pltpu.VMEM((heads, span, NOPE + LANES), BF16),
                pltpu.VMEM((heads, VDIM + 16, span), F32),
                pltpu.VMEM((heads, 8, span), F32),
                pltpu.VMEM((span, heads * VDIM), BF16),
                pltpu.VMEM((2, pieces, rows, width // pieces), BF16),
                pltpu.VMEM((2, pieces, rows, width // pieces), BF16),
                pltpu.VMEM((2, pieces, rows, width // pieces), F32),
                pltpu.VMEM((pieces, rows, width // pieces), BF16),
                pltpu.VMEM((pieces, rows, width // pieces), BF16),
                pltpu.VMEM(uv.shape[::-1], BF16),
                pltpu.VMEM((span, heads * NOPE), BF16),
                pltpu.VMEM((heads * VDIM, span), BF16),
                pltpu.VMEM((span, LANES), F32),
                pltpu.VMEM((span, LANES), F32),
                dma(2 * chunks + 7),
                dma(8 * O),
                dma(S * T),
                dma(3),
                dma(T),
                dma(2 * pieces),
                dma(2 * pieces),
                dma(pieces),
                dma(pieces),
            ],
            compiler_params=pltpu.CompilerParams(
                collective_id=0, has_side_effects=True, vmem_limit_bytes=60 * 1024 * 1024
            ),
        )(
            tokens, dq, dl, dr.T, qg.reshape(1, -1), lg.reshape(1, -1),
            uq, ur, uk, uv, ow, *tables,
        )
        return total.astype(BF16)

    return jax.shard_map(
        local,
        mesh=mesh,
        in_specs=(
            P(("sp", "tp"), None),
            P(),
            P(),
            P(),
            P(),
            P(),
            P(None, "tp"),
            P(None, "tp"),
            P(None, "tp"),
            P(None, "tp"),
            P("tp", None),
        ),
        out_specs=P(("sp", "tp"), None),
        check_vma=False,
    )
```

profile of v0, /device:TPU:120, one launch (start us, length us, event | category | flops | bytes accessed | tf_op | source)
XLA Modules:
  0.0 206.3 jit_solution(13309881958611178168)
XLA Ops:
  0.0 204.2 %shard_map.145 = f32[64,4096]{1,0:T(8,128)} custom-call(bf16[64,4096]{1,0:T(8,128)(2,1)} %tokens_hbm.1, bf16[4096,1024]{1,0:T(8,128)(2,1)} %dq_hbm.1, bf16[4096,512]{1,0:T(8,128)(2,1)} %dl_hbm.1, bf16[64,4096]{1,0:T(8,128)(2,1)} %bitcast.3, f32[1,1024]{1,0:T(1,128)} %bitcast.4, f32[1,512]{1,0:T(1,128)} %bitcast.5, bf16[1024,512]{1,0:T(8,128)(2,1)} %uq_hbm.1, ...), custom_call_target="tpu_custom_call" | custom-call | tf_op jit(solution)/shard_map/pallas_call | solution.py:464
  204.2 2.1 %convert_element_type.3 = bf16[64,4096]{1,0:T(8,128)(2,1)} convert(f32[64,4096]{1,0:T(8,128)} %shard_map.145) | non-fusion elementwise | flops 262144 | bytes 1572864 | tf_op jit(solution)/shard_map/convert_element_type | solution.py:512
where the time goes:
time: 206 us
  Pallas kernels  204 us (99%)
  other arithmetic  2.07 us (1%)
    pallas_call x1, Pallas kernels, local(): pl.pallas_call(functools.partial(kernel, S, T, chunks, pieces), out_shape...  204 us

commit v1 on v0

--- a/solution.py
+++ b/solution.py
@@ -17,6 +17,12 @@
 norm_eps = 1e-06
 masked_score = -1e30
 log2e = 1.4426950408889634
+
+EVENTS = [
+    (0, 0), (3, 0), (1, 0), (0, 3), (0, 1), (2, 0), (3, 3), (1, 3),
+    (3, 1), (1, 1), (0, 2), (2, 3), (2, 1), (3, 2), (1, 2), (2, 2),
+]
+AHEAD = 2
 
 MESH = pl.DeviceIdType.MESH
 F32 = jnp.float32
@@ -88,8 +94,12 @@
     cos_ref,
     sin_ref,
     load_sem,
+    line_send,
+    line_recv,
     kv_send,
     kv_recv,
+    beside_send,
+    beside_recv,
     q_send,
     q_recv,
     pair_send,
@@ -107,6 +117,8 @@
     tp = lax.axis_index("tp")
     o, i = sp // 2, sp % 2
     g, c = tp // 2, tp % 2
+    Y = int(O**0.5)
+    z, y = o // Y, o % Y
 
     def dev(o_, i_, g_, c_):
         return {"sp": o_ * 2 + i_, "tp": g_ * 2 + c_}
@@ -132,30 +144,102 @@
     ow_load = load(ow_hbm, ow)
 
     barrier = pltpu.get_barrier_semaphore()
-    for d in range(1, O):
-        pl.semaphore_signal(barrier, inc=1, device_id=dev((o + d) % O, i, g, c), device_id_type=MESH)
-    for target in (across, beside, mate):
-        pl.semaphore_signal(barrier, inc=1, device_id=target, device_id_type=MESH)
-
-    def block(o_, i_, g_, c_):
-        return (o_ * 2 + i_) * T + g_ * 2 + c_
+    for step_ in (1, Y - 1):
+        for node_ in (z * Y + (y + step_) % Y, (z + step_) % Y * Y + y):
+            pl.semaphore_signal(barrier, inc=1, device_id={"sp": node_ * 2 + i, "tp": tp}, device_id_type=MESH)
+    for n in range(1, T):
+        pl.semaphore_signal(barrier, inc=1, device_id={"sp": sp, "tp": (tp + n) % T}, device_id_type=MESH)
+    pl.semaphore_signal(barrier, inc=1, device_id=beside, device_id_type=MESH)
 
     def block_rows(b):
         return pl.ds(pl.multiple_of(b * rows, rows), rows)
 
-    def kv_copy(b, target, index):
-        part = kv.at[block_rows(b)]
+    mine = block_rows(sp * T + tp)
+    half = span // 2
+    first_pos = jnp.where(i == 0, y, z)
+    second_pos = jnp.where(i == 0, z, y)
+
+    def node(da, db, i_):
+        a_ = (jnp.where(i_ == 0, y, z) + da) % Y
+        b_ = (jnp.where(i_ == 0, z, y) + db) % Y
+        return jnp.where(i_ == 0, b_ * Y + a_, a_ * Y + b_)
+
+    def send(part, target, send_sem, recv_sem):
         return pltpu.make_async_remote_copy(
             src_ref=part,
             dst_ref=part,
-            send_sem=kv_send.at[index],
-            recv_sem=kv_recv.at[b],
+            send_sem=send_sem,
+            recv_sem=recv_sem,
             device_id=target,
             device_id_type=MESH,
         )
 
-    def kv_wait(b):
-        kv_copy(b, mate, 0).wait_recv()
+    def near(t):
+        return {"sp": o * 2 + i, "tp": t}
+
+    def ring(da, db):
+        return {"sp": node(da, db, i) * 2 + i, "tp": tp}
+
+    def line_copy(n):
+        return send(kv.at[mine], near((tp + n) % T), line_send.at[n], line_recv.at[tp])
+
+    def line_wait(n):
+        t = (tp + n) % T
+        part = kv.at[block_rows(sp * T + t)]
+        send(part, near(t), line_send.at[n], line_recv.at[t]).wait_recv()
+
+    def half_part(s, h):
+        return kv.at[pl.ds(pl.multiple_of(s * span + h * half, half), half)]
+
+    def half_copy(s, h, target, index):
+        return send(half_part(s, h), target, kv_send.at[index], kv_recv.at[s * 2 + h])
+
+    def half_wait(s, h):
+        half_copy(s, h, beside, 0).wait_recv()
+
+    def beside_copy(s, index):
+        part = kv.at[pl.ds(pl.multiple_of(s * span, span), span)]
+        return send(part, beside, beside_send.at[index], beside_recv.at[s])
+
+    def steps(k):
+        da = db = 0
+        for n, (p, q) in enumerate(EVENTS):
+            da = jnp.where(k == n, p, da)
+            db = jnp.where(k == n, q, db)
+        return da, db
+
+    def first_ring(act):
+        for h in range(2):
+            act(half_copy(sp, h, ring(1, 0), h))
+            act(half_copy(sp, 1 - h, ring(Y - 1, 0), 2 + h))
+
+    def second_ring(s, da, act):
+        for h in range(2):
+            act(half_copy(s, h, ring(0, 1), 4 + da * 4 + h))
+            act(half_copy(s, 1 - h, ring(0, Y - 1), 4 + da * 4 + 2 + h))
+
+    def relay(s, k, da, db):
+        along = jnp.where(db == 0, da, db)
+        way = jnp.where(along == 1, Y - 1, 1)
+        h = jnp.where(along == 1, 1, 0)
+        target = ring(jnp.where(db == 0, way, 0), jnp.where(db == 0, 0, way))
+        return along, h, half_copy(s, h, target, 4 + 4 * Y + k)
+
+    def forward(k):
+        da, db = steps(k)
+        s = node(da, db, i) * 2 + i
+        along, h, copy = relay(s, k, da, db)
+        half_wait(s, h)
+        pl.when(along != 2)(copy.start)
+        half_wait(s, 1 - h)
+        pl.when(db == 0)(lambda: second_ring(s, da, start))
+        beside_copy(s, k).start()
+
+    def start(copy):
+        copy.start()
+
+    def sent(copy):
+        copy.wait_send()
 
     start_cos, start_sin = base_cos[pl.ds(sp, 1), :], base_sin[pl.ds(sp, 1), :]
     sign = jnp.where(lax.broadcasted_iota(jnp.int32, (1, LANES), 1) % ROPE < ROPE // 2, -1.0, 1.0)
@@ -171,82 +255,12 @@
     turned = dot_nt(tokens[...], dr[...])
     turned = jnp.concatenate([turned, jnp.zeros((rows, LANES - ROPE), F32)], axis=1)
     own_rows = pl.ds(pl.multiple_of(tp * rows, rows), rows)
-    mine = block_rows(block(o, i, g, c))
     kv[mine, :rank] = normed(latent, lg_ref[...]).astype(BF16)
     kv[mine, rank:] = turn(turned, cos_ref[own_rows, :], sin_ref[own_rows, :]).astype(BF16)
 
-    pl.semaphore_wait(barrier, O - 1 + 3)
-
-    def up_copy(d):
-        return kv_copy(block(o, i, g, c), dev((o + d) % O, i, g, c), d)
-
-    def relay_near(d, act):
-        b = block(o - d, i, g, c)
-        act(kv_copy(b, across, O + d))
-
-        @pl.when((i == 0) | (d > 0))
-        def _():
-            act(kv_copy(b, beside, 2 * O + 2 * d))
-
-        act(kv_copy(b, mate, 4 * O + 4 * d))
-
-    def relay_far(d, act):
-        b = block(o - d, i, 1 - g, c)
-
-        @pl.when(((i == 0) | (d > 0)) & (d < O - 1))
-        def _():
-            act(kv_copy(b, beside, 2 * O + 2 * d + 1))
-
-        act(kv_copy(b, mate, 4 * O + 4 * d + 1))
-
-    def relay_beside(d, act):
-        b = block(o - d, 1 - i, g, c)
-
-        @pl.when(d == O - 1)
-        def _():
-            act(kv_copy(b, across, 2 * O + 2 * d + 1))
-
-        act(kv_copy(b, mate, 4 * O + 4 * d + 2))
-
-    def relay_corner(d, act):
-        act(kv_copy(block(o - d, 1 - i, 1 - g, c), mate, 4 * O + 4 * d + 3))
-
-    def start(copy):
-        copy.start()
-
-    def sent(copy):
-        copy.wait_send()
-
-    def near(d):
-        kv_wait(block(o - d, i, g, c))
-        relay_near(d, start)
-
-    def far(d):
-        kv_wait(block(o - d, i, 1 - g, c))
-        relay_far(d, start)
-
-    def beside_in(d):
-        kv_wait(block(o - d, 1 - i, g, c))
-        relay_beside(d, start)
-
-    def corner_in(d):
-        kv_wait(block(o - d, 1 - i, 1 - g, c))
-        relay_corner(d, start)
-
-    def each(first, body):
-        def run(d, carry):
-            body(d)
-            return carry
-
-        lax.fori_loop(first, o + 1, run, 0)
-
-    for d in range(1, O):
-
-        @pl.when(o + d < O)
-        def _(d=d):
-            up_copy(d).start()
-
-    relay_near(0, start)
+    pl.semaphore_wait(barrier, 4 + T - 1 + 1)
+    for n in range(1, T):
+        line_copy(n).start()
 
     query = jnp.zeros((rows, dq.shape[1]), F32)
     for k in range(chunks):
@@ -254,21 +268,20 @@
         query += dot(tokens[:, k * step : (k + 1) * step], dq[k * step : (k + 1) * step, :])
     ql[own_rows, :] = normed(query, qg_ref[...]).astype(BF16)
 
-    def q_copy(t, target, index):
-        part = ql.at[block_rows(t)]
-        return pltpu.make_async_remote_copy(
-            src_ref=part,
-            dst_ref=part,
-            send_sem=q_send.at[index],
-            recv_sem=q_recv.at[t],
-            device_id=target,
-            device_id_type=MESH,
-        )
-
-    other = (1 - g) * 2 + c
-    q_copies = [q_copy(tp, across, 0), q_copy(tp, mate, 1), q_copy(other, mate, 2)]
-    q_copies[0].start()
-    q_copies[1].start()
+    def q_copy(n):
+        return send(ql.at[own_rows], near((tp + n) % T), q_send.at[n], q_recv.at[tp])
+
+    def q_wait(n):
+        t = (tp + n) % T
+        send(ql.at[block_rows(t)], near(t), q_send.at[n], q_recv.at[t]).wait_recv()
+
+    for n in range(1, T):
+        q_copy(n).start()
+    for n in range(1, T):
+        line_wait(n)
+    first_ring(start)
+    second_ring(sp, 0, start)
+    beside_copy(sp, 0).start()
 
     def kv_heads(s):
         part = pl.ds(pl.multiple_of(s * span, span), span)
@@ -278,25 +291,9 @@
     up_loads[2].wait()
     up_loads[3].wait()
     uvt[...] = uv[...].T
-    far(0)
-    pl.when(o >= 1)(lambda: near(1))
-    kv_wait(block(o, i, g, 1 - c))
-    kv_wait(block(o, i, 1 - g, 1 - c))
     first_keys[...], first_values[...] = kv_heads(sp)
-    each(2, near)
-
-    q_copy(other, mate, 2).wait_recv()
-    q_copies[2].start()
-
-    @pl.when(i == 1)
-    def _():
-        beside_in(0)
-        corner_in(0)
-
-    q_copy(g * 2 + 1 - c, mate, 0).wait_recv()
-    q_copy((1 - g) * 2 + 1 - c, mate, 0).wait_recv()
-
-    pl.when(o >= 1)(lambda: far(1))
+    for n in range(1, T):
+        q_wait(n)
     for copy in up_loads[:2]:
         copy.wait()
     scale = (NOPE + ROPE) ** (-0.5) * log2e
@@ -339,25 +336,26 @@
             acc[h] = acc[h] * jnp.exp2(old - new) + dot(value, weights)
             best[h] = jnp.broadcast_to(new, best.shape[1:])
 
-    def next_to(d):
-        kv_wait(block(o - d, 1 - i, g, 1 - c))
-        kv_wait(block(o - d, 1 - i, 1 - g, 1 - c))
-        attend((o - d) * 2 + 1 - i)
-
-    def column(d):
-        pl.when(d + 3 <= o)(lambda: far(d + 3))
-        kv_wait(block(o - d, i, g, 1 - c))
-        kv_wait(block(o - d, i, 1 - g, 1 - c))
-        attend((o - d) * 2 + i)
-        corner_in(d)
-
-    pl.when(o >= 2)(lambda: far(2))
+    def partner(k):
+        da, db = steps(k)
+        o_ = node(da, db, 1 - i)
+        s = o_ * 2 + 1 - i
+        beside_copy(s, k).wait_recv()
+        pl.when(s < sp)(lambda: attend(s))
+
+    def column(k, carry):
+        pl.when(k + AHEAD < len(EVENTS))(lambda: forward(k + AHEAD))
+        da, db = steps(k)
+        o_ = node(da, db, i)
+        pl.when(o_ < o)(lambda: attend(o_ * 2 + i))
+        partner(k)
+        return carry
+
     attend(sp, masked=True)
-    pl.when(o >= 3)(lambda: far(3))
-    each(1, beside_in)
-    pl.when(i == 1)(lambda: next_to(0))
-    each(1, column)
-    each(1, next_to)
+    for k in range(1, 1 + AHEAD):
+        forward(k)
+    partner(0)
+    lax.fori_loop(1, len(EVENTS), column, 0)
 
     for h in range(heads):
         whole = acc[h]
@@ -414,26 +412,22 @@
         total = kept[1, j] + pair_in[1, j].astype(F32) + cross_in[j].astype(F32)
         out_ref[:, j * width : (j + 1) * width] = total
 
-    for d in range(1, O):
-
-        @pl.when(o + d < O)
-        def _(d=d):
-            up_copy(d).wait_send()
-
-    def drain(d, carry):
-        relay_near(d, sent)
-        relay_far(d, sent)
-
-        @pl.when((i == 1) | (d > 0))
-        def _():
-            relay_beside(d, sent)
-            relay_corner(d, sent)
-
+    def drain(k, carry):
+        da, db = steps(k)
+        s = node(da, db, i) * 2 + i
+        along, h, copy = relay(s, k, da, db)
+        pl.when(along != 2)(copy.wait_send)
+        pl.when(db == 0)(lambda: second_ring(s, da, sent))
+        beside_copy(s, k).wait_send()
         return carry
 
-    lax.fori_loop(0, o + 1, drain, 0)
-    for copy in q_copies:
-        copy.wait_send()
+    lax.fori_loop(1, len(EVENTS), drain, 0)
+    first_ring(sent)
+    second_ring(sp, 0, sent)
+    beside_copy(sp, 0).wait_send()
+    for n in range(1, T):
+        line_copy(n).wait_send()
+        q_copy(n).wait_send()
     for j in range(pieces):
         pair_copy(0, j).wait_send()
         pair_copy(1, j).wait_send()
@@ -442,7 +436,7 @@
 
 def solution(mesh):
     S, T = mesh.shape["sp"], mesh.shape["tp"]
-    assert S % 2 == 0 and T == 4
+    assert S == 32 and T == 4
 
     def local(tokens, dq, dl, dr, qg, lg, uq, ur, uk, uv, ow):
         rows, depth = tokens.shape
@@ -493,9 +487,13 @@
                 pltpu.VMEM((span, LANES), F32),
                 pltpu.VMEM((span, LANES), F32),
                 dma(2 * chunks + 7),
-                dma(8 * O),
-                dma(S * T),
-                dma(3),
+                dma(T),
+                dma(T),
+                dma(4 + 4 * 4 + O),
+                dma(2 * S),
+                dma(O),
+                dma(S),
+                dma(T),
                 dma(T),
                 dma(2 * pieces),
                 dma(2 * pieces),

time: 206 us -> 94.6 us (0.46)
  the two profiles are of different devices: /device:TPU:120 before, /device:TPU:122 now
where the time goes in v1:
time: 94.6 us; the launch traced here: 94.4 us
  Pallas kernels  92.3 us (98%)
  other arithmetic  2.07 us (2%)
    pallas_call x1, Pallas kernels, local(): pl.pallas_call(functools.partial(kernel, S, T, chunks, pieces), out_shape...  92.3 us
    convert_element_type x1, other arithmetic, local(): return total.astype(BF16)  2.07 us

profile of v1, /device:TPU:122, one launch (start us, length us, event | category | flops | bytes accessed | tf_op | source)
XLA Modules:
  0.0 94.4 jit_solution(9678275541508302591)
XLA Ops:
  0.0 92.3 %shard_map.145 = f32[64,4096]{1,0:T(8,128)} custom-call(bf16[64,4096]{1,0:T(8,128)(2,1)} %tokens_hbm.1, bf16[4096,1024]{1,0:T(8,128)(2,1)} %dq_hbm.1, bf16[4096,512]{1,0:T(8,128)(2,1)} %dl_hbm.1, bf16[64,4096]{1,0:T(8,128)(2,1)} %bitcast.3, f32[1,1024]{1,0:T(1,128)} %bitcast.4, f32[1,512]{1,0:T(1,128)} %bitcast.5, bf16[1024,512]{1,0:T(8,128)(2,1)} %uq_hbm.1, ...), custom_call_target="tpu_custom_call" | custom-call | tf_op jit(solution)/shard_map/pallas_call | solution.py:458
  92.3 2.1 %convert_element_type.3 = bf16[64,4096]{1,0:T(8,128)(2,1)} convert(f32[64,4096]{1,0:T(8,128)} %shard_map.145) | non-fusion elementwise | flops 262144 | bytes 1572864 | tf_op jit(solution)/shard_map/convert_element_type | solution.py:510

commit v2 on v1

--- a/solution.py
+++ b/solution.py
@@ -83,11 +83,11 @@
     acc,
     best,
     att,
-    pair_out,
-    pair_in,
+    side_out,
+    side_in,
     kept,
-    cross_out,
-    cross_in,
+    pass_out,
+    pass_in,
     uvt,
     first_keys,
     first_values,
@@ -102,10 +102,10 @@
     beside_recv,
     q_send,
     q_recv,
-    pair_send,
-    pair_recv,
-    cross_send,
-    cross_recv,
+    side_send,
+    side_recv,
+    pass_send,
+    pass_recv,
 ):
     O = S // 2
     rows = tokens.shape[0]
@@ -116,16 +116,9 @@
     sp = lax.axis_index("sp")
     tp = lax.axis_index("tp")
     o, i = sp // 2, sp % 2
-    g, c = tp // 2, tp % 2
     Y = int(O**0.5)
     z, y = o // Y, o % Y
-
-    def dev(o_, i_, g_, c_):
-        return {"sp": o_ * 2 + i_, "tp": g_ * 2 + c_}
-
-    across = dev(o, i, 1 - g, c)
-    beside = dev(o, 1 - i, g, c)
-    mate = dev(o, i, g, 1 - c)
+    beside = {"sp": o * 2 + 1 - i, "tp": tp}
 
     step = depth // chunks
     loads = []
@@ -363,54 +356,51 @@
 
     ow_load.wait()
     width = ow.shape[1] // pieces
-    lag = min(3, pieces)
-
-    def pair_copy(phase, j):
+    opposite, right, left = (tp + 2) % T, (tp + 1) % T, (tp + T - 1) % T
+
+    def exchange(out, into, target, send_sem, recv_sem):
         return pltpu.make_async_remote_copy(
-            src_ref=pair_out.at[phase, j],
-            dst_ref=pair_in.at[phase, j],
-            send_sem=pair_send.at[phase * pieces + j],
-            recv_sem=pair_recv.at[phase * pieces + j],
-            device_id=mate,
+            src_ref=out,
+            dst_ref=into,
+            send_sem=send_sem,
+            recv_sem=recv_sem,
+            device_id=near(target),
             device_id_type=MESH,
         )
 
-    def cross_copy(j):
-        return pltpu.make_async_remote_copy(
-            src_ref=cross_out.at[j],
-            dst_ref=cross_in.at[j],
-            send_sem=cross_send.at[j],
-            recv_sem=cross_recv.at[j],
-            device_id=across,
-            device_id_type=MESH,
-        )
-
-    def project(phase, group, j):
-        top = att[block_rows(group * 2 + 1 - c), :]
-        low_part = att[block_rows(group * 2 + c), :]
-        part = dot(jnp.concatenate([top, low_part], axis=0), ow[:, j * width : (j + 1) * width])
-        pair_out[phase, j] = part[:rows].astype(BF16)
-        kept[phase, j] = part[rows:]
-        pair_copy(phase, j).start()
-
-    def cross(j):
-        pair_copy(0, j).wait_recv()
-        cross_out[j] = (kept[0, j] + pair_in[0, j].astype(F32)).astype(BF16)
-        cross_copy(j).start()
-
-    for j in range(pieces):
-        project(0, 1 - g, j)
-        if j >= lag:
-            cross(j - lag)
-    for j in range(pieces - lag, pieces):
-        cross(j)
-    for j in range(pieces):
-        project(1, g, j)
-    for j in range(pieces):
-        pair_copy(1, j).wait_recv()
-        cross_copy(j).wait_recv()
-        total = kept[1, j] + pair_in[1, j].astype(F32) + cross_in[j].astype(F32)
-        out_ref[:, j * width : (j + 1) * width] = total
+    def pass_copy(j):
+        target = right if j < pieces // 2 else left
+        return exchange(pass_out.at[j], pass_in.at[j], target, pass_send.at[j], pass_recv.at[j])
+
+    def side_copy(side, j):
+        n = side * pieces + j
+        target = (right, left)[side]
+        return exchange(side_out.at[side, j], side_in.at[side, j], target, side_send.at[n], side_recv.at[n])
+
+    attended = jnp.concatenate([att[block_rows(t), :] for t in (opposite, right, left, tp)], axis=0)
+    for n in range(pieces):
+        j = n // 2 + n % 2 * (pieces // 2)
+        late = 0 if j < pieces // 2 else 1
+        part = dot(attended, ow[:, j * width : (j + 1) * width])
+        pass_out[j] = part[:rows].astype(BF16)
+        pass_copy(j).start()
+        kept[0, j] = part[(1 + late) * rows : (2 + late) * rows]
+        side_out[1 - late, j] = part[(2 - late) * rows : (3 - late) * rows].astype(BF16)
+        kept[1, j] = part[3 * rows :]
+    order = [n // 2 + n % 2 * (pieces // 2) for n in range(pieces)]
+    for j in order:
+        late = 0 if j < pieces // 2 else 1
+        side_copy(1 - late, j).start()
+    for j in order:
+        late = 0 if j < pieces // 2 else 1
+        pass_copy(j).wait_recv()
+        side_out[late, j] = (kept[0, j] + pass_in[j].astype(F32)).astype(BF16)
+        side_copy(late, j).start()
+    for j in order:
+        side_copy(0, j).wait_recv()
+        side_copy(1, j).wait_recv()
+        total = kept[1, j] + side_in[0, j].astype(F32) + side_in[1, j].astype(F32)
+        out_ref[:, j * width : (j + 1) * width] = total.astype(BF16)
 
     def drain(k, carry):
         da, db = steps(k)
@@ -429,9 +419,9 @@
         line_copy(n).wait_send()
         q_copy(n).wait_send()
     for j in range(pieces):
-        pair_copy(0, j).wait_send()
-        pair_copy(1, j).wait_send()
-        cross_copy(j).wait_send()
+        pass_copy(j).wait_send()
+        side_copy(0, j).wait_send()
+        side_copy(1, j).wait_send()
 
 
 def solution(mesh):
@@ -457,7 +447,7 @@
         like = lambda a: pltpu.VMEM(a.shape, a.dtype)
         total = pl.pallas_call(
             functools.partial(kernel, S, T, chunks, pieces),
-            out_shape=jax.ShapeDtypeStruct((rows, width), F32),
+            out_shape=jax.ShapeDtypeStruct((rows, width), BF16),
             in_specs=[hbm, hbm, hbm, hbm, vmem, vmem, hbm, hbm, hbm, hbm, hbm, vmem, vmem, vmem, vmem],
             out_specs=vmem,
             scratch_shapes=[
@@ -507,7 +497,7 @@
             tokens, dq, dl, dr.T, qg.reshape(1, -1), lg.reshape(1, -1),
             uq, ur, uk, uv, ow, *tables,
         )
-        return total.astype(BF16)
+        return total
 
     return jax.shard_map(
         local,

time: 94.6 us -> 77.6 us (0.82)
  the two profiles are of different devices: /device:TPU:122 before, /device:TPU:126 now
where the time goes in v2:
time: 77.6 us; the launch traced here: 77.4 us
  Pallas kernels  75.5 us (97%)
  local copies, waits for them, and re-layouts  1.87 us (2%)
    pallas_call x1, Pallas kernels, local(): pl.pallas_call(functools.partial(kernel, S, T, chunks, pieces), out_shape...  75.5 us
    unnamed x1, local copies, waits for them, and re-layouts  1.87 us

profile of v2, /device:TPU:126, one launch (start us, length us, event | category | flops | bytes accessed | tf_op | source)
XLA Modules:
  0.0 77.4 jit_solution(8579077022323844486)
XLA Ops:
  0.0 75.5 %shard_map.145 = bf16[64,4096]{1,0:T(8,128)(2,1)} custom-call(bf16[64,4096]{1,0:T(8,128)(2,1)} %tokens_hbm.1, bf16[4096,1024]{1,0:T(8,128)(2,1)} %dq_hbm.1, bf16[4096,512]{1,0:T(8,128)(2,1)} %dl_hbm.1, bf16[64,4096]{1,0:T(8,128)(2,1)} %bitcast.3, f32[1,1024]{1,0:T(1,128)} %bitcast.4, f32[1,512]{1,0:T(1,128)} %bitcast.5, bf16[1024,512]{1,0:T(8,128)(2,1)} %uq_hbm.1, ...), custom_call_target="tpu_custom_call" | custom-call | tf_op jit(solution)/shard_map/pallas_call | solution.py:448
  75.5 1.9 %copy.17 = bf16[64,4096]{1,0:T(8,128)(2,1)} copy(bf16[64,4096]{1,0:T(8,128)(2,1)} %shard_map.145) | data formatting | bytes 1048576

commit v3 on v2

--- a/solution.py
+++ b/solution.py
@@ -67,7 +67,7 @@
     base_sin,
     row_cos,
     row_sin,
-    out_ref,
+    out_hbm,
     tokens,
     dq,
     dl,
@@ -89,11 +89,15 @@
     pass_out,
     pass_in,
     uvt,
-    first_keys,
-    first_values,
+    keys_a,
+    values_a,
+    keys_b,
+    values_b,
     cos_ref,
     sin_ref,
+    out,
     load_sem,
+    out_sem,
     line_send,
     line_recv,
     kv_send,
@@ -173,13 +177,34 @@
     def ring(da, db):
         return {"sp": node(da, db, i) * 2 + i, "tp": tp}
 
-    def line_copy(n):
-        return send(kv.at[mine], near((tp + n) % T), line_send.at[n], line_recv.at[tp])
-
-    def line_wait(n):
-        t = (tp + n) % T
-        part = kv.at[block_rows(sp * T + t)]
-        send(part, near(t), line_send.at[n], line_recv.at[t]).wait_recv()
+    def line_part(ref, first, t, h):
+        size = rows if h is None else rows // 2
+        start_ = first + t * rows + (0 if h is None else h * size)
+        return ref.at[pl.ds(pl.multiple_of(start_, size), size)]
+
+    def around(ref, first, send_sem, recv_sem):
+        ways = (1, T - 1)
+
+        def own(n, act):
+            part = line_part(ref, first, tp, None)
+            act(send(part, near((tp + ways[n]) % T), send_sem.at[n], recv_sem.at[n]))
+
+        def relay_on(n, act):
+            part = line_part(ref, first, (tp + T - ways[n]) % T, n)
+            act(send(part, near((tp + ways[n]) % T), send_sem.at[2 + n], recv_sem.at[2 + n]))
+
+        def close_wait(n):
+            t = (tp + T - ways[n]) % T
+            send(line_part(ref, first, t, None), near(t), send_sem.at[n], recv_sem.at[n]).wait_recv()
+
+        def far_wait(n):
+            t = (tp + T // 2) % T
+            send(line_part(ref, first, t, n), near(t), send_sem.at[2 + n], recv_sem.at[2 + n]).wait_recv()
+
+        return own, relay_on, close_wait, far_wait
+
+    kv_line = around(kv, sp * span, line_send, line_recv)
+    q_line = around(ql, 0, q_send, q_recv)
 
     def half_part(s, h):
         return kv.at[pl.ds(pl.multiple_of(s * span + h * half, half), half)]
@@ -252,8 +277,8 @@
     kv[mine, rank:] = turn(turned, cos_ref[own_rows, :], sin_ref[own_rows, :]).astype(BF16)
 
     pl.semaphore_wait(barrier, 4 + T - 1 + 1)
-    for n in range(1, T):
-        line_copy(n).start()
+    for n in range(2):
+        kv_line[0](n, start)
 
     query = jnp.zeros((rows, dq.shape[1]), F32)
     for k in range(chunks):
@@ -261,32 +286,38 @@
         query += dot(tokens[:, k * step : (k + 1) * step], dq[k * step : (k + 1) * step, :])
     ql[own_rows, :] = normed(query, qg_ref[...]).astype(BF16)
 
-    def q_copy(n):
-        return send(ql.at[own_rows], near((tp + n) % T), q_send.at[n], q_recv.at[tp])
-
-    def q_wait(n):
-        t = (tp + n) % T
-        send(ql.at[block_rows(t)], near(t), q_send.at[n], q_recv.at[t]).wait_recv()
-
-    for n in range(1, T):
-        q_copy(n).start()
-    for n in range(1, T):
-        line_wait(n)
+    for n in range(2):
+        kv_line[2](n)
+        kv_line[1](n, start)
+    for n in range(2):
+        q_line[0](n, start)
+    for n in range(2):
+        kv_line[3](n)
     first_ring(start)
     second_ring(sp, 0, start)
     beside_copy(sp, 0).start()
 
-    def kv_heads(s):
-        part = pl.ds(pl.multiple_of(s * span, span), span)
-        lat = kv[part, :rank]
-        return dot(lat, uk[...]).astype(BF16), dot_nt(uvt[...], lat).astype(BF16)
+    def key_rows(s):
+        return pl.ds(pl.multiple_of(s * span, span), span)
+
+    def project_keys(keys, n, s):
+        keys[n * span : (n + 1) * span, :] = dot(kv[key_rows(s), :rank], uk[...]).astype(BF16)
+
+    def project_values(values, n, s):
+        values[:, n * span : (n + 1) * span] = dot_nt(uvt[...], kv[key_rows(s), :rank]).astype(BF16)
 
     up_loads[2].wait()
     up_loads[3].wait()
     uvt[...] = uv[...].T
-    first_keys[...], first_values[...] = kv_heads(sp)
-    for n in range(1, T):
-        q_wait(n)
+    beside_copy(sp + 1 - 2 * i, 0).wait_recv()
+    for n, s in enumerate((sp, sp + 1 - 2 * i)):
+        project_keys(keys_a, n, s)
+        project_values(values_a, n, s)
+    for n in range(2):
+        q_line[2](n)
+        q_line[1](n, start)
+    for n in range(2):
+        q_line[3](n)
     for copy in up_loads[:2]:
         copy.wait()
     scale = (NOPE + ROPE) ** (-0.5) * log2e
@@ -302,53 +333,74 @@
         best[h] = jnp.full(best.shape[1:], masked_score, F32)
         acc[h] = jnp.zeros(acc.shape[1:], F32)
 
-    def attend(s, masked=False):
-        rot = kv[pl.ds(pl.multiple_of(s * span, span), span), rank:]
-        keys, values = (first_keys[...], first_values[...]) if masked else kv_heads(s)
-        ones = jnp.ones((acc.shape[1] - VDIM, span), BF16)
+    def pair_of(k):
+        da, db = steps(k)
+        own_, other_ = node(da, db, i) * 2 + i, node(da, db, 1 - i) * 2 + 1 - i
+        return own_, other_
+
+    def attend(keys, values, s, ahead_keys, ahead_values, ahead, masked=False):
+        use = [t < sp for t in s]
+        rot = jnp.concatenate([kv[key_rows(t), rank:] for t in s], axis=0)
+        ones = jnp.ones((acc.shape[1] - VDIM, 2 * span), BF16)
         if masked:
+            use[0] = sp >= 0
             k_pos = lax.broadcasted_iota(jnp.int32, (span, span), 0)
             q_pos = lax.broadcasted_iota(jnp.int32, (span, span), 1)
             allowed = k_pos <= q_pos
+        penalty = [jnp.where(u, 0.0, -masked_score) for u in use]
+        floor = [jnp.where(u, -masked_score, masked_score) for u in use]
 
         def score(h):
             key = jnp.concatenate([keys[:, h * NOPE : (h + 1) * NOPE], rot], axis=1)
             return dot_nt(key, qh[h])
 
-        ahead = score(0)
+        later = score(0)
         for h in range(heads):
-            scores = ahead
+            scores = later
             if h + 1 < heads:
-                ahead = score(h + 1)
-            value = jnp.concatenate([values[h * VDIM : (h + 1) * VDIM], ones], axis=0)
+                later = score(h + 1)
+            if ahead is not None:
+                if h % 2 == 0:
+                    project_keys(ahead_keys, h // 2, ahead[h // 2])
+                else:
+                    project_values(ahead_values, h // 2, ahead[h // 2])
+            value = jnp.concatenate([values[h * VDIM : (h + 1) * VDIM, :], ones], axis=0)
+            parts = [scores[:span], scores[span:]]
             if masked:
-                scores = jnp.where(allowed, scores, masked_score)
+                parts[0] = jnp.where(allowed, parts[0], masked_score)
             old = best[h][:1]
-            new = jnp.maximum(old, jnp.max(scores, axis=0, keepdims=True))
-            weights = jnp.exp2(scores - new).astype(BF16)
-            acc[h] = acc[h] * jnp.exp2(old - new) + dot(value, weights)
+            new = old
+            for part, limit in zip(parts, floor):
+                new = jnp.maximum(new, jnp.minimum(jnp.max(part, axis=0, keepdims=True), limit))
+            weights = [jnp.exp2(part - (new + extra)).astype(BF16) for part, extra in zip(parts, penalty)]
+            acc[h] = acc[h] * jnp.exp2(old - new) + dot(value, jnp.concatenate(weights, axis=0))
             best[h] = jnp.broadcast_to(new, best.shape[1:])
 
-    def partner(k):
-        da, db = steps(k)
-        o_ = node(da, db, 1 - i)
-        s = o_ * 2 + 1 - i
-        beside_copy(s, k).wait_recv()
-        pl.when(s < sp)(lambda: attend(s))
-
-    def column(k, carry):
+    buffers = [(keys_a, values_a), (keys_b, values_b)]
+
+    def arrive(k):
         pl.when(k + AHEAD < len(EVENTS))(lambda: forward(k + AHEAD))
-        da, db = steps(k)
-        o_ = node(da, db, i)
-        pl.when(o_ < o)(lambda: attend(o_ * 2 + i))
-        partner(k)
+        beside_copy(pair_of(k + 1)[1], 0).wait_recv()
+
+    def step(k, slot):
+        arrive(k)
+        now, later = pair_of(k), pair_of(k + 1)
+        any_ = (now[0] < sp) | (now[1] < sp) | (later[0] < sp) | (later[1] < sp)
+        pl.when(any_)(lambda: attend(*buffers[slot], now, *buffers[1 - slot], later))
+
+    for k in range(1, AHEAD):
+        forward(k)
+    arrive(0)
+    attend(*buffers[0], (sp, sp + 1 - 2 * i), *buffers[1], pair_of(1), masked=True)
+
+    def column(m, carry):
+        step(2 * m + 1, 1)
+        step(2 * m + 2, 0)
         return carry
 
-    attend(sp, masked=True)
-    for k in range(1, 1 + AHEAD):
-        forward(k)
-    partner(0)
-    lax.fori_loop(1, len(EVENTS), column, 0)
+    lax.fori_loop(0, len(EVENTS) // 2 - 1, column, 0)
+    last = pair_of(len(EVENTS) - 1)
+    pl.when((last[0] < sp) | (last[1] < sp))(lambda: attend(*buffers[1], last, None, None, None))
 
     for h in range(heads):
         whole = acc[h]
@@ -396,11 +448,17 @@
         pass_copy(j).wait_recv()
         side_out[late, j] = (kept[0, j] + pass_in[j].astype(F32)).astype(BF16)
         side_copy(late, j).start()
+
+    def out_copy(j):
+        part = pl.ds(j * width, width)
+        return pltpu.make_async_copy(out.at[:, part], out_hbm.at[:, part], out_sem.at[j])
+
     for j in order:
         side_copy(0, j).wait_recv()
         side_copy(1, j).wait_recv()
         total = kept[1, j] + side_in[0, j].astype(F32) + side_in[1, j].astype(F32)
-        out_ref[:, j * width : (j + 1) * width] = total.astype(BF16)
+        out[:, j * width : (j + 1) * width] = total.astype(BF16)
+        out_copy(j).start()
 
     def drain(k, carry):
         da, db = steps(k)
@@ -415,10 +473,12 @@
     first_ring(sent)
     second_ring(sp, 0, sent)
     beside_copy(sp, 0).wait_send()
-    for n in range(1, T):
-        line_copy(n).wait_send()
-        q_copy(n).wait_send()
+    for line in (kv_line, q_line):
+        for n in range(2):
+            line[0](n, sent)
+            line[1](n, sent)
     for j in range(pieces):
+        out_copy(j).wait()
         pass_copy(j).wait_send()
         side_copy(0, j).wait_send()
         side_copy(1, j).wait_send()
@@ -449,7 +509,7 @@
             functools.partial(kernel, S, T, chunks, pieces),
             out_shape=jax.ShapeDtypeStruct((rows, width), BF16),
             in_specs=[hbm, hbm, hbm, hbm, vmem, vmem, hbm, hbm, hbm, hbm, hbm, vmem, vmem, vmem, vmem],
-            out_specs=vmem,
+            out_specs=hbm,
             scratch_shapes=[
                 like(tokens),
                 like(dq),
@@ -472,11 +532,15 @@
                 pltpu.VMEM((pieces, rows, width // pieces), BF16),
                 pltpu.VMEM((pieces, rows, width // pieces), BF16),
                 pltpu.VMEM(uv.shape[::-1], BF16),
-                pltpu.VMEM((span, heads * NOPE), BF16),
-                pltpu.VMEM((heads * VDIM, span), BF16),
+                pltpu.VMEM((2 * span, heads * NOPE), BF16),
+                pltpu.VMEM((heads * VDIM, 2 * span), BF16),
+                pltpu.VMEM((2 * span, heads * NOPE), BF16),
+                pltpu.VMEM((heads * VDIM, 2 * span), BF16),
                 pltpu.VMEM((span, LANES), F32),
                 pltpu.VMEM((span, LANES), F32),
+                pltpu.VMEM((rows, width), BF16),
                 dma(2 * chunks + 7),
+                dma(pieces),
                 dma(T),
                 dma(T),
                 dma(4 + 4 * 4 + O),

time: 77.6 us -> 72.7 us (0.937)
  the two profiles are of different devices: /device:TPU:126 before, /device:TPU:65 now
where the time goes in v3:
time: 72.7 us; the launch traced here: 72.3 us
  Pallas kernels  70.5 us (97%)
  local copies, waits for them, and re-layouts  1.87 us (3%)
    pallas_call x1, Pallas kernels, local(): pl.pallas_call(functools.partial(kernel, S, T, chunks, pieces), out_shape...  70.5 us
    unnamed x1, local copies, waits for them, and re-layouts  1.87 us

profile of v3, /device:TPU:65, one launch (start us, length us, event | category | flops | bytes accessed | tf_op | source)
XLA Modules:
  0.0 72.3 jit_solution(9704947182003068908)
XLA Ops:
  0.0 70.5 %shard_map.145 = bf16[64,4096]{1,0:T(8,128)(2,1)} custom-call(bf16[64,4096]{1,0:T(8,128)(2,1)} %tokens_hbm.1, bf16[4096,1024]{1,0:T(8,128)(2,1)} %dq_hbm.1, bf16[4096,512]{1,0:T(8,128)(2,1)} %dl_hbm.1, bf16[64,4096]{1,0:T(8,128)(2,1)} %bitcast.3, f32[1,1024]{1,0:T(1,128)} %bitcast.4, f32[1,512]{1,0:T(1,128)} %bitcast.5, bf16[1024,512]{1,0:T(8,128)(2,1)} %uq_hbm.1, ...), custom_call_target="tpu_custom_call" | custom-call | tf_op jit(solution)/shard_map/pallas_call | solution.py:508
  70.5 1.9 %copy.17 = bf16[64,4096]{1,0:T(8,128)(2,1)} copy(bf16[64,4096]{1,0:T(8,128)(2,1)} %shard_map.145) | data formatting | bytes 1048576

commit v4 on v3

v4 whole, which is shorter than its diff:
```python
import functools

import jax
import jax.numpy as jnp
import numpy as np
from jax import lax
from jax.experimental import pallas as pl
from jax.experimental.pallas import tpu as pltpu
from jax.sharding import PartitionSpec as P

NOPE = 128
ROPE = 64
VDIM = 128
LANES = 128

rope_base = 500000.0
norm_eps = 1e-06
masked_score = -1e30
log2e = 1.4426950408889634

EVENTS = [
    (0, 0), (3, 0), (1, 0), (0, 3), (0, 1), (3, 3), (1, 3), (3, 1),
    (1, 1), (2, 0), (0, 2), (2, 3), (2, 1), (3, 2), (1, 2), (2, 2),
]
FAR = 9
NEXT = (11, 12)
PASS = {3: (11,), 4: (12,), 7: (15,)}
START = {3: (15,)}
SENT = 60
LEAD = 4
SENT_HALVES = 30

MESH = pl.DeviceIdType.MESH
F32 = jnp.float32
BF16 = jnp.bfloat16


def dot(a, b):
    return jnp.dot(a, b, preferred_element_type=F32)


def dot_nt(a, b):
    return lax.dot_general(a, b, (((1,), (1,)), ((), ())), preferred_element_type=F32)


def turn(v, cosine, sine):
    lane = lax.broadcasted_iota(jnp.int32, v.shape, 1)
    other = jnp.where(lane % ROPE < ROPE // 2, pltpu.roll(v, LANES - ROPE // 2, 1), pltpu.roll(v, ROPE // 2, 1))
    return v * cosine + other * sine


def normed(v, gain):
    return v * lax.rsqrt(jnp.mean(v * v, axis=-1, keepdims=True) + norm_eps) * gain


def kernel(
    S,
    T,
    chunks,
    pieces,
    tokens_hbm,
    dq_hbm,
    dl_hbm,
    dr_hbm,
    qg_hbm,
    lg_hbm,
    uq_hbm,
    ur_hbm,
    uk_hbm,
    uv_hbm,
    ow_hbm,
    base_hbm,
    turn_hbm,
    out_hbm,
    tokens,
    dq,
    dl,
    dr,
    uq,
    ur,
    uk,
    uv,
    ow,
    kv,
    ql,
    qh,
    acc,
    best,
    att,
    side_out,
    side_in,
    kept,
    pass_out,
    pass_in,
    uvt,
    keys_a,
    values_a,
    keys_b,
    values_b,
    keys_in,
    values_in,
    scores_a,
    scores_b,
    best_a,
    best_b,
    cos_ref,
    sin_ref,
    out,
    qg_ref,
    lg_ref,
    base,
    turns,
    load_sem,
    out_sem,
    line_send,
    line_recv,
    kv_send,
    kv_recv,
    share_send,
    share_recv,
    q_send,
    q_recv,
    side_send,
    side_recv,
    pass_send,
    pass_recv,
):
    O = S // 2
    rows = tokens.shape[0]
    span = rows * T
    depth = tokens.shape[1]
    heads = qh.shape[0]
    rank = dl.shape[1]
    sp = lax.axis_index("sp")
    tp = lax.axis_index("tp")
    o, i = sp // 2, sp % 2
    Y = int(O**0.5)
    z, y = o // Y, o % Y
    beside = {"sp": o * 2 + 1 - i, "tp": tp}

    step = depth // chunks
    loads = []

    def load(src, dst):
        copy = pltpu.make_async_copy(src, dst, load_sem.at[len(loads)])
        loads.append(copy)
        copy.start()
        return copy

    tok_load = load(tokens_hbm, tokens)
    small_loads = [load(lg_hbm, lg_ref), load(base_hbm, base), load(turn_hbm, turns), load(qg_hbm, qg_ref)]
    dl_loads = [load(dl_hbm.at[pl.ds(k * step, step)], dl.at[pl.ds(k * step, step)]) for k in range(chunks)]
    dr_load = load(dr_hbm, dr)
    dq_loads = [load(dq_hbm.at[pl.ds(k * step, step)], dq.at[pl.ds(k * step, step)]) for k in range(chunks)]
    barrier = pltpu.get_barrier_semaphore()
    for step_ in (1, Y - 1):
        for node_ in (z * Y + (y + step_) % Y, (z + step_) % Y * Y + y):
            pl.semaphore_signal(barrier, inc=1, device_id={"sp": node_ * 2 + i, "tp": tp}, device_id_type=MESH)
    for n in range(1, T):
        pl.semaphore_signal(barrier, inc=1, device_id={"sp": sp, "tp": (tp + n) % T}, device_id_type=MESH)
    pl.semaphore_signal(barrier, inc=1, device_id=beside, device_id_type=MESH)

    def block_rows(b):
        return pl.ds(pl.multiple_of(b * rows, rows), rows)

    mine = block_rows(o * T + tp)
    first_pos = jnp.where(i == 0, y, z)
    second_pos = jnp.where(i == 0, z, y)

    def node(da, db, i_):
        a_ = (jnp.where(i_ == 0, y, z) + da) % Y
        b_ = (jnp.where(i_ == 0, z, y) + db) % Y
        return jnp.where(i_ == 0, b_ * Y + a_, a_ * Y + b_)

    def send(part, target, send_sem, recv_sem):
        return pltpu.make_async_remote_copy(
            src_ref=part,
            dst_ref=part,
            send_sem=send_sem,
            recv_sem=recv_sem,
            device_id=target,
            device_id_type=MESH,
        )

    def near(t):
        return {"sp": o * 2 + i, "tp": t}

    def ring(da, db):
        return {"sp": node(da, db, i) * 2 + i, "tp": tp}

    def line_part(ref, first, t, h):
        size = rows if h is None else rows // 2
        start_ = first + t * rows + (0 if h is None else h * size)
        return ref.at[pl.ds(pl.multiple_of(start_, size), size)]

    def around(ref, first, send_sem, recv_sem):
        ways = (1, T - 1)

        def own(n):
            part = line_part(ref, first, tp, None)
            send(part, near((tp + ways[n]) % T), send_sem.at[0], recv_sem.at[n]).start()

        def relay_on(n):
            part = line_part(ref, first, (tp + T - ways[n]) % T, n)
            send(part, near((tp + ways[n]) % T), send_sem.at[0], recv_sem.at[2 + n]).start()

        def close_wait(n):
            t = (tp + T - ways[n]) % T
            send(line_part(ref, first, t, None), near(t), send_sem.at[0], recv_sem.at[n]).wait_recv()

        def far_wait(n):
            t = (tp + T // 2) % T
            send(line_part(ref, first, t, n), near(t), send_sem.at[0], recv_sem.at[2 + n]).wait_recv()

        return own, relay_on, close_wait, far_wait

    kv_line = around(kv, o * span, line_send, line_recv)
    q_line = around(ql, 0, q_send, q_recv)

    def sub_copy(n, t, target):
        part = kv.at[block_rows(n * T + t)]
        return send(part, target, kv_send.at[0], kv_recv.at[n * T + t])

    def sub_wait(n, t):
        sub_copy(n, t, beside).wait_recv()

    def steps(k):
        da = db = 0
        for n, (p, q) in enumerate(EVENTS):
            da = jnp.where(k == n, p, da)
            db = jnp.where(k == n, q, db)
        return da, db

    def beyond(j):
        return (tp + j) % T

    def first_ring(t):
        for way in (1, Y - 1):
            sub_copy(o, t, ring(way, 0)).start()

    def second_ring(n, t):
        for way in (1, Y - 1):
            sub_copy(n, t, ring(0, way)).start()

    def place(k):
        da, db = steps(k)
        return da, db, node(da, db, i)

    def early(k):
        da, db, n = place(k)
        sub_wait(n, tp)
        second_ring(n, tp)
        pl.when((i == 0) == (da == Y - 1))(sub_copy(n, tp, ring((Y - da) % Y, 0)).start)

    def rest(k):
        n = place(k)[2]
        for j in (1, 3, 2):
            sub_wait(n, beyond(j))
            second_ring(n, beyond(j))

    def whole(k):
        da, db, n = place(k)
        for j in (0, 1, 3, 2):
            sub_wait(n, beyond(j))
            way = Y - 1 if j in (3, 2) else 1
            pl.when(db == Y - way)(sub_copy(n, beyond(j), ring(0, way)).start)

    def cross_start(k):
        da, db, n = place(k)
        sub_wait(n, tp)
        pl.when(db == 0)(lambda: second_ring(n, tp))
        pl.when(db == jnp.where(i == 0, Y - 1, 1))(sub_copy(n, tp, ring(0, (Y - db) % Y)).start)
        for way in (1, T - 1):
            sub_copy(n, tp, near(beyond(way))).start()

    def cross_pass(k):
        da, db, n = place(k)
        for way in (1, T - 1):
            sub_wait(n, beyond(T - way))
        way = jnp.where((db + i) % 2 == 0, 1, T - 1)
        sub_copy(n, (tp + T - way) % T, near((tp + way) % T)).start()

    def cross_end(k):
        sub_wait(place(k)[2], beyond(2))

    tok_load.wait()
    latent = jnp.zeros((rows, rank), F32)
    for k in range(chunks):
        dl_loads[k].wait()
        latent += dot(tokens[:, k * step : (k + 1) * step], dl[k * step : (k + 1) * step, :])
    dr_load.wait()
    for copy in small_loads:
        copy.wait()
    start_cos, start_sin = base[0, pl.ds(sp, 1), :], base[1, pl.ds(sp, 1), :]
    sign = jnp.where(lax.broadcasted_iota(jnp.int32, (1, LANES), 1) % ROPE < ROPE // 2, -1.0, 1.0)
    cos_ref[...] = start_cos * turns[0] - start_sin * turns[1]
    sin_ref[...] = (start_sin * turns[0] + start_cos * turns[1]) * sign
    turned = dot_nt(tokens[...], dr[...])
    turned = jnp.concatenate([turned, jnp.zeros((rows, LANES - ROPE), F32)], axis=1)
    own_rows = pl.ds(pl.multiple_of(tp * rows, rows), rows)
    kv[mine, :rank] = normed(latent, lg_ref[...]).astype(BF16)
    kv[mine, rank:] = turn(turned, cos_ref[own_rows, :], sin_ref[own_rows, :]).astype(BF16)

    up_loads = [load(uq_hbm, uq), load(ur_hbm, ur), load(uk_hbm, uk), load(uv_hbm, uv)]
    ow_load = load(ow_hbm, ow)
    pl.semaphore_wait(barrier, 4 + T - 1 + 1)
    for n in range(2):
        kv_line[0](n)
    first_ring(tp)
    second_ring(o, tp)

    query = jnp.zeros((rows, dq.shape[1]), F32)
    for k in range(chunks):
        dq_loads[k].wait()
        query += dot(tokens[:, k * step : (k + 1) * step], dq[k * step : (k + 1) * step, :])
    ql[own_rows, :] = normed(query, qg_ref[...]).astype(BF16)

    early(1)
    early(2)
    for n in range(2):
        kv_line[2](n)
        kv_line[1](n)
    for n in range(2):
        q_line[0](n)
    for j in (1, 3):
        first_ring(beyond(j))
        second_ring(o, beyond(j))
    for n in range(2):
        kv_line[3](n)
    first_ring(beyond(2))
    second_ring(o, beyond(2))

    def spot(k):
        n = node(*steps(k), i)
        return pl.ds(pl.multiple_of(n * span, span), span)

    def project_keys(k, parity):
        keys = own_keys[parity]
        keys[k // 2, :, : heads * NOPE] = dot(kv[spot(k), :rank], uk[...]).astype(BF16)
        keys[k // 2, :, heads * NOPE :] = kv[spot(k), rank:]

    def project_values(k, parity):
        own_values[parity][k // 2] = dot_nt(uvt[...], kv[spot(k), :rank]).astype(BF16)

    own_keys, own_values = (keys_a, keys_b), (values_a, values_b)
    kept_scores, kept_best = (scores_a, scores_b), (best_a, best_b)

    def share(n, k, parity):
        own, into = ((own_keys, keys_in), (own_values, values_in))[n]
        return pltpu.make_async_remote_copy(
            src_ref=own[parity].at[k // 2],
            dst_ref=into.at[k],
            send_sem=share_send.at[n],
            recv_sem=share_recv.at[n * O + k],
            device_id=beside,
            device_id_type=MESH,
        )

    def prepare_keys(k):
        project_keys(k, k % 2)
        share(0, k, k % 2).start()

    def prepare_values(k):
        project_values(k, k % 2)
        share(1, k, k % 2).start()

    up_loads[2].wait()
    up_loads[3].wait()
    uvt[...] = uv[...].T
    prepare_keys(0)
    prepare_values(0)
    cross_start(FAR)
    for n in range(2):
        q_line[2](n)
        q_line[1](n)
    for k in range(1, 3):
        rest(k)
        prepare_keys(k)
        prepare_values(k)
    cross_pass(FAR)
    for n in range(2):
        q_line[3](n)
    for copy in up_loads[:2]:
        copy.wait()
    scale = (NOPE + ROPE) ** (-0.5) * log2e
    plain = (dot(ql[...], uq[...]) * scale).astype(BF16)
    turning = dot(ql[...], ur[...]) * scale
    low = lax.broadcasted_iota(jnp.int32, (span, LANES), 1) < ROPE
    for pair in range(heads // 2):
        both = turn(turning[:, pair * LANES : (pair + 1) * LANES], cos_ref[...], sin_ref[...])
        qh[2 * pair, :, NOPE:] = jnp.where(low, both, 0.0).astype(BF16)
        qh[2 * pair + 1, :, NOPE:] = jnp.where(low, pltpu.roll(both, ROPE, 1), 0.0).astype(BF16)
    for h in range(heads):
        qh[h, :, :NOPE] = plain[:, h * NOPE : (h + 1) * NOPE]
        best[h] = jnp.full(best.shape[1:], masked_score, F32)
        acc[h] = jnp.zeros(acc.shape[1:], F32)

    def used(k):
        first = k == 0
        mine_, other_ = node(*steps(k), i), node(*steps(k), 1 - i)
        return (mine_ < o) | first, (other_ < o) | (first & (i == 1))

    def score(k, parity, h, masked=False):
        keys = own_keys[parity]
        part = slice(h * NOPE, (h + 1) * NOPE)
        rot = jnp.concatenate([keys[k // 2, :, heads * NOPE :], keys_in[k, :, heads * NOPE :]], axis=0)
        key = jnp.concatenate([keys[k // 2, :, part], keys_in[k, :, part]], axis=0)
        scores = dot_nt(jnp.concatenate([key, rot], axis=1), qh[h])
        pieces_ = [scores[:span], scores[span:]]
        if masked:
            k_pos = lax.broadcasted_iota(jnp.int32, (span, span), 0)
            q_pos = lax.broadcasted_iota(jnp.int32, (span, span), 1)
            pieces_[0] = jnp.where(k_pos <= q_pos, pieces_[0], masked_score)
        top = None
        for n, (piece, use) in enumerate(zip(pieces_, used(k))):
            kept_scores[parity][h, n * span : (n + 1) * span, :] = piece
            limit = jnp.where(use, -masked_score, masked_score)
            new = jnp.minimum(jnp.max(piece, axis=0, keepdims=True), limit)
            top = new if top is None else jnp.maximum(top, new)
        kept_best[parity][h] = jnp.broadcast_to(top, best.shape[1:])

    ones = jnp.ones((acc.shape[1] - VDIM, 2 * span), BF16)

    def weigh(k, parity, h):
        part = slice(h * VDIM, (h + 1) * VDIM)
        value = jnp.concatenate([own_values[parity][k // 2, part, :], values_in[k, part, :]], axis=1)
        value = jnp.concatenate([value, ones], axis=0)
        old = best[h][:1]
        new = jnp.maximum(old, kept_best[parity][h][:1])
        weights = []
        for n, use in enumerate(used(k)):
            shift = new + jnp.where(use, 0.0, -masked_score)
            weights.append(jnp.exp2(kept_scores[parity][h, n * span : (n + 1) * span, :] - shift).astype(BF16))
        acc[h] = acc[h] * jnp.exp2(old - new) + dot(value, jnp.concatenate(weights, axis=0))
        best[h] = jnp.broadcast_to(new, best.shape[1:])

    count = len(EVENTS)

    def step(k, parity, scoring=True, keying=True, valuing=True):
        if keying:
            far = steps(k + LEAD)[0] == Y // 2
            pl.when(far)(lambda: cross_end(k + LEAD))
            pl.when(~far)(lambda: whole(k + LEAD))
            for table, act in ((PASS, cross_pass), (START, cross_start)):
                for n, events in table.items():
                    if n % 2 == parity:
                        pl.when(k == n)(lambda events=events, act=act: [act(e) for e in events][0])
        if scoring:
            share(0, k + 1, 1 - parity).wait_recv()
        share(1, k, parity).wait_recv()
        needed = used(k)[0] | used(k)[1]
        if scoring:
            needed = needed | used(k + 1)[0] | used(k + 1)[1]

        @pl.when(needed)
        def _():
            for h in range(heads):
                if scoring:
                    score(k + 1, 1 - parity, h)
                if keying and h == 0:
                    project_keys(k + LEAD, parity)
                if valuing and h == 2:
                    project_values(k + LEAD - 1, 1 - parity)
                weigh(k, parity, h)

        @pl.when(~needed)
        def _():
            if keying:
                project_keys(k + LEAD, parity)
            if valuing:
                project_values(k + LEAD - 1, 1 - parity)

        if keying:
            share(0, k + LEAD, parity).start()
        if valuing:
            share(1, k + LEAD - 1, 1 - parity).start()

    share(0, 0, 0).wait_recv()
    for h in range(heads):
        score(0, 0, h, masked=True)
    for k in NEXT:
        cross_start(k)
    whole(3)
    prepare_keys(3)

    def column(m, carry):
        step(2 * m, 0)
        step(2 * m + 1, 1)
        return carry

    lax.fori_loop(0, (count - LEAD) // 2, column, 0)
    for k in range(count - LEAD, count):
        step(k, k % 2, scoring=k + 1 < count, keying=k + LEAD < count, valuing=k + LEAD - 1 < count)

    for h in range(heads):
        whole = acc[h]
        att[:, h * VDIM : (h + 1) * VDIM] = (whole[:VDIM] / whole[VDIM : VDIM + 1]).T.astype(BF16)

    ow_load.wait()
    width = ow.shape[1] // pieces
    opposite, right, left = (tp + 2) % T, (tp + 1) % T, (tp + T - 1) % T

    def exchange(out, into, target, send_sem, recv_sem):
        return pltpu.make_async_remote_copy(
            src_ref=out,
            dst_ref=into,
            send_sem=send_sem,
            recv_sem=recv_sem,
            device_id=near(target),
            device_id_type=MESH,
        )

    def pass_copy(j):
        target = right if j < pieces // 2 else left
        return exchange(pass_out.at[j], pass_in.at[j], target, pass_send.at[0], pass_recv.at[j])

    def side_copy(side, j):
        n = side * pieces + j
        target = (right, left)[side]
        return exchange(side_out.at[side, j], side_in.at[side, j], target, side_send.at[0], side_recv.at[n])

    attended = jnp.concatenate([att[block_rows(t), :] for t in (opposite, right, left, tp)], axis=0)
    for n in range(pieces):
        j = n // 2 + n % 2 * (pieces // 2)
        late = 0 if j < pieces // 2 else 1
        part = dot(attended, ow[:, j * width : (j + 1) * width])
        pass_out[j] = part[:rows].astype(BF16)
        pass_copy(j).start()
        kept[0, j] = part[(1 + late) * rows : (2 + late) * rows]
        side_out[1 - late, j] = part[(2 - late) * rows : (3 - late) * rows].astype(BF16)
        kept[1, j] = part[3 * rows :]
    order = [n // 2 + n % 2 * (pieces // 2) for n in range(pieces)]
    for j in order:
        late = 0 if j < pieces // 2 else 1
        side_copy(1 - late, j).start()
    for j in order:
        late = 0 if j < pieces // 2 else 1
        pass_copy(j).wait_recv()
        side_out[late, j] = (kept[0, j] + pass_in[j].astype(F32)).astype(BF16)
        side_copy(late, j).start()

    def out_copy(j):
        part = pl.ds(j * width, width)
        return pltpu.make_async_copy(out.at[:, part], out_hbm.at[:, part], out_sem.at[0])

    for j in order:
        side_copy(0, j).wait_recv()
        side_copy(1, j).wait_recv()
        total = kept[1, j] + side_in[0, j].astype(F32) + side_in[1, j].astype(F32)
        out[:, j * width : (j + 1) * width] = total.astype(BF16)
        out_copy(j).start()

    def all_sent(ref, send_sem):
        send(ref, beside, send_sem.at[0], send_sem.at[0]).wait_send()

    all_sent(kv.at[pl.ds(0, SENT * rows)], kv_send)
    for n, refs in enumerate((own_keys, own_values)):
        for ref in refs:
            send(ref, beside, share_send.at[n], share_send.at[n]).wait_send()
    all_sent(kv.at[pl.ds(0, 3 * rows)], line_send)
    all_sent(ql.at[pl.ds(0, 3 * rows)], q_send)
    all_sent(side_out, side_send)
    all_sent(pass_out, pass_send)
    pltpu.make_async_copy(out, out_hbm, out_sem.at[0]).wait()


def solution(mesh):
    S, T = mesh.shape["sp"], mesh.shape["tp"]
    assert S == 32 and T == 4

    def local(tokens, dq, dl, dr, qg, lg, uq, ur, uk, uv, ow):
        rows, depth = tokens.shape
        span = rows * T
        heads = uk.shape[1] // NOPE
        width = ow.shape[1]
        rank = dl.shape[1]
        chunks, pieces = 4, 8
        inverse = np.float32(rope_base) ** (-np.arange(0, ROPE, 2, dtype=np.float32) / np.float32(ROPE))
        inverse = np.tile(inverse.astype(np.float64), LANES // (ROPE // 2))
        starts = np.arange(S)[:, None] * span * inverse
        steps = np.arange(span)[:, None] * inverse
        tables = [jnp.asarray(np.stack([np.cos(a), np.sin(a)]), F32) for a in (starts, steps)]
        O = S // 2
        hbm = pl.BlockSpec(memory_space=pl.ANY)
        dma = lambda n: pltpu.SemaphoreType.DMA((n,))
        like = lambda a: pltpu.VMEM(a.shape, a.dtype)
        total = pl.pallas_call(
            functools.partial(kernel, S, T, chunks, pieces),
            out_shape=jax.ShapeDtypeStruct((rows, width), BF16),
            in_specs=[hbm] * 13,
            out_specs=hbm,
            scratch_shapes=[
                like(tokens),
                like(dq),
                like(dl),
                pltpu.VMEM(dr.shape[::-1], dr.dtype),
                like(uq),
                like(ur),
                like(uk),
                like(uv),
                like(ow),
                pltpu.VMEM((O * span, rank + LANES), BF16),
                pltpu.VMEM((span, dq.shape[1]), BF16),
                pltpu.VMEM((heads, span, NOPE + LANES), BF16),
                pltpu.VMEM((heads, VDIM + 16, span), F32),
                pltpu.VMEM((heads, 8, span), F32),
                pltpu.VMEM((span, heads * VDIM), BF16),
                pltpu.VMEM((2, pieces, rows, width // pieces), BF16),
                pltpu.VMEM((2, pieces, rows, width // pieces), BF16),
                pltpu.VMEM((2, pieces, rows, width // pieces), F32),
                pltpu.VMEM((pieces, rows, width // pieces), BF16),
                pltpu.VMEM((pieces, rows, width // pieces), BF16),
                pltpu.VMEM(uv.shape[::-1], BF16),
                pltpu.VMEM((O // 2, span, heads * NOPE + LANES), BF16),
                pltpu.VMEM((O // 2, heads * VDIM, span), BF16),
                pltpu.VMEM((O // 2, span, heads * NOPE + LANES), BF16),
                pltpu.VMEM((O // 2, heads * VDIM, span), BF16),
                pltpu.VMEM((O, span, heads * NOPE + LANES), BF16),
                pltpu.VMEM((O, heads * VDIM, span), BF16),
                pltpu.VMEM((heads, 2 * span, span), F32),
                pltpu.VMEM((heads, 2 * span, span), F32),
                pltpu.VMEM((heads, 8, span), F32),
                pltpu.VMEM((heads, 8, span), F32),
                pltpu.VMEM((span, LANES), F32),
                pltpu.VMEM((span, LANES), F32),
                pltpu.VMEM((rows, width), BF16),
                pltpu.VMEM((1, dq.shape[1]), F32),
                pltpu.VMEM((1, rank), F32),
                pltpu.VMEM(tables[0].shape, F32),
                pltpu.VMEM(tables[1].shape, F32),
                dma(2 * chunks + 13),
                dma(1),
                dma(1),
                dma(4),
                dma(1),
                dma(T * O),
                dma(2),
                dma(2 * O),
                dma(1),
                dma(4),
                dma(1),
                dma(2 * pieces),
                dma(1),
                dma(pieces),
            ],
            compiler_params=pltpu.CompilerParams(
                collective_id=0, has_side_effects=True, vmem_limit_bytes=63 * 1024 * 1024
            ),
        )(
            tokens, dq, dl, dr.T, qg.reshape(1, -1), lg.reshape(1, -1),
            uq, ur, uk, uv, ow, *tables,
        )
        return total

    return jax.shard_map(
        local,
        mesh=mesh,
        in_specs=(
            P(("sp", "tp"), None),
            P(),
            P(),
            P(),
            P(),
            P(),
            P(None, "tp"),
            P(None, "tp"),
            P(None, "tp"),
            P(None, "tp"),
            P("tp", None),
        ),
        out_specs=P(("sp", "tp"), None),
        check_vma=False,
    )
```

time: 72.7 us -> 63.9 us (0.88)
  Pallas kernels: 70.5 us -> 61.7 us
    pallas_call x1, Pallas kernels: 70.5 us -> 61.7 us  [local(): pl.pallas_call(functools.partial(kernel, S, T, chunks, pieces), out_shape...]
where the time goes in v4:
time: 63.9 us; the launch traced here: 63.6 us
  Pallas kernels  61.7 us (97%)
  local copies, waits for them, and re-layouts  1.87 us (3%)
    pallas_call x1, Pallas kernels, local(): pl.pallas_call(functools.partial(kernel, S, T, chunks, pieces), out_shape...  61.7 us
    unnamed x1, local copies, waits for them, and re-layouts  1.87 us

profile of v4, /device:TPU:65, one launch (start us, length us, event | category | flops | bytes accessed | tf_op | source)
XLA Modules:
  0.0 63.6 jit_solution(17349041670073729324)
XLA Ops:
  0.0 61.7 %shard_map.127 = bf16[64,4096]{1,0:T(8,128)(2,1)} custom-call(bf16[64,4096]{1,0:T(8,128)(2,1)} %tokens_hbm.1, bf16[4096,1024]{1,0:T(8,128)(2,1)} %dq_hbm.1, bf16[4096,512]{1,0:T(8,128)(2,1)} %dl_hbm.1, bf16[64,4096]{1,0:T(8,128)(2,1)} %bitcast.3, f32[1,1024]{1,0:T(1,128)} %bitcast.4, f32[1,512]{1,0:T(1,128)} %bitcast.5, bf16[1024,512]{1,0:T(8,128)(2,1)} %uq_hbm.1, ...), custom_call_target="tpu_custom_call" | custom-call | tf_op jit(solution)/shard_map/pallas_call | solution.py:587
  61.7 1.9 %copy.15 = bf16[64,4096]{1,0:T(8,128)(2,1)} copy(bf16[64,4096]{1,0:T(8,128)(2,1)} %shard_map.127) | data formatting | bytes 1048576

commit v5 on v4

--- a/solution.py
+++ b/solution.py
@@ -71,7 +71,7 @@
     ow_hbm,
     base_hbm,
     turn_hbm,
-    out_hbm,
+    out_ref,
     tokens,
     dq,
     dl,
@@ -105,13 +105,11 @@
     best_b,
     cos_ref,
     sin_ref,
-    out,
     qg_ref,
     lg_ref,
     base,
     turns,
     load_sem,
-    out_sem,
     line_send,
     line_recv,
     kv_send,
@@ -225,11 +223,7 @@
         sub_copy(n, t, beside).wait_recv()
 
     def steps(k):
-        da = db = 0
-        for n, (p, q) in enumerate(EVENTS):
-            da = jnp.where(k == n, p, da)
-            db = jnp.where(k == n, q, db)
-        return da, db
+        return EVENTS[k]
 
     def beyond(j):
         return (tp + j) % T
@@ -250,7 +244,7 @@
         da, db, n = place(k)
         sub_wait(n, tp)
         second_ring(n, tp)
-        pl.when((i == 0) == (da == Y - 1))(sub_copy(n, tp, ring((Y - da) % Y, 0)).start)
+        pl.when(i == (0 if da == Y - 1 else 1))(sub_copy(n, tp, ring((Y - da) % Y, 0)).start)
 
     def rest(k):
         n = place(k)[2]
@@ -263,13 +257,16 @@
         for j in (0, 1, 3, 2):
             sub_wait(n, beyond(j))
             way = Y - 1 if j in (3, 2) else 1
-            pl.when(db == Y - way)(sub_copy(n, beyond(j), ring(0, way)).start)
+            if db == Y - way:
+                sub_copy(n, beyond(j), ring(0, way)).start()
 
     def cross_start(k):
         da, db, n = place(k)
         sub_wait(n, tp)
-        pl.when(db == 0)(lambda: second_ring(n, tp))
-        pl.when(db == jnp.where(i == 0, Y - 1, 1))(sub_copy(n, tp, ring(0, (Y - db) % Y)).start)
+        if db == 0:
+            second_ring(n, tp)
+        if db in (1, Y - 1):
+            pl.when(i == (0 if db == Y - 1 else 1))(sub_copy(n, tp, ring(0, Y - db)).start)
         for way in (1, T - 1):
             sub_copy(n, tp, near(beyond(way))).start()
 
@@ -282,6 +279,17 @@
 
     def cross_end(k):
         sub_wait(place(k)[2], beyond(2))
+
+    def needs(k):
+        da, db, n = place(k)
+        return n < o, node(da, db, 1 - i) < o
+
+    def is_late(k):
+        da, db = steps(k)
+        return da == Y // 2 or (k >= LEAD and db == Y // 2)
+
+    def finish(k):
+        cross_end(k) if steps(k)[0] == Y // 2 else whole(k)
 
     tok_load.wait()
     latent = jnp.zeros((rows, rank), F32)
@@ -331,7 +339,8 @@
     second_ring(o, beyond(2))
 
     def spot(k):
-        n = node(*steps(k), i)
+        n = place(k)[2]
+        n = jnp.where(needs(k)[0], n, o) if k >= LEAD else n
         return pl.ds(pl.multiple_of(n * span, span), span)
 
     def project_keys(k, parity):
@@ -373,11 +382,10 @@
     for n in range(2):
         q_line[2](n)
         q_line[1](n)
-    for k in range(1, 3):
-        rest(k)
-        prepare_keys(k)
-        prepare_values(k)
-    cross_pass(FAR)
+    rest(1)
+    rest(2)
+    prepare_keys(1)
+    prepare_values(1)
     for n in range(2):
         q_line[3](n)
     for copy in up_loads[:2]:
@@ -396,15 +404,18 @@
         acc[h] = jnp.zeros(acc.shape[1:], F32)
 
     def used(k):
-        first = k == 0
-        mine_, other_ = node(*steps(k), i), node(*steps(k), 1 - i)
-        return (mine_ < o) | first, (other_ < o) | (first & (i == 1))
+        return (sp >= 0, i == 1) if k == 0 else needs(k)
+
+    def slots(k):
+        mine_, other_ = used(k)
+        return (jnp.where(mine_, k // 2, 0), jnp.where(other_, k, 0)) if k >= LEAD - 1 else (k // 2, k)
 
     def score(k, parity, h, masked=False):
         keys = own_keys[parity]
         part = slice(h * NOPE, (h + 1) * NOPE)
-        rot = jnp.concatenate([keys[k // 2, :, heads * NOPE :], keys_in[k, :, heads * NOPE :]], axis=0)
-        key = jnp.concatenate([keys[k // 2, :, part], keys_in[k, :, part]], axis=0)
+        own_, in_ = slots(k)
+        rot = jnp.concatenate([keys[own_, :, heads * NOPE :], keys_in[in_, :, heads * NOPE :]], axis=0)
+        key = jnp.concatenate([keys[own_, :, part], keys_in[in_, :, part]], axis=0)
         scores = dot_nt(jnp.concatenate([key, rot], axis=1), qh[h])
         pieces_ = [scores[:span], scores[span:]]
         if masked:
@@ -423,7 +434,8 @@
 
     def weigh(k, parity, h):
         part = slice(h * VDIM, (h + 1) * VDIM)
-        value = jnp.concatenate([own_values[parity][k // 2, part, :], values_in[k, part, :]], axis=1)
+        own_, in_ = slots(k)
+        value = jnp.concatenate([own_values[parity][own_, part, :], values_in[in_, part, :]], axis=1)
         value = jnp.concatenate([value, ones], axis=0)
         old = best[h][:1]
         new = jnp.maximum(old, kept_best[parity][h][:1])
@@ -436,18 +448,30 @@
 
     count = len(EVENTS)
 
-    def step(k, parity, scoring=True, keying=True, valuing=True):
+    def when(condition, act):
+        pl.when(condition)(act)
+
+    def step(k):
+        parity = k % 2
+        scoring, keying, valuing = k + 1 < count, k + LEAD < count, k + LEAD - 1 < count
+        wants = [needs(k + LEAD)[0] if keying else None, needs(k + LEAD - 1)[0] if valuing else None]
         if keying:
-            far = steps(k + LEAD)[0] == Y // 2
-            pl.when(far)(lambda: cross_end(k + LEAD))
-            pl.when(~far)(lambda: whole(k + LEAD))
+            if is_late(k + LEAD):
+                when(wants[0], lambda: finish(k + LEAD))
+            else:
+                finish(k + LEAD)
             for table, act in ((PASS, cross_pass), (START, cross_start)):
-                for n, events in table.items():
-                    if n % 2 == parity:
-                        pl.when(k == n)(lambda events=events, act=act: [act(e) for e in events][0])
+                for e in table.get(k, ()):
+                    act(e)
         if scoring:
-            share(0, k + 1, 1 - parity).wait_recv()
-        share(1, k, parity).wait_recv()
+            if k + 1 < LEAD:
+                share(0, k + 1, 1 - parity).wait_recv()
+            else:
+                when(needs(k + 1)[1], share(0, k + 1, 1 - parity).wait_recv)
+        if k < LEAD - 1:
+            share(1, k, parity).wait_recv()
+        else:
+            when(needs(k)[1], share(1, k, parity).wait_recv)
         needed = used(k)[0] | used(k)[1]
         if scoring:
             needed = needed | used(k + 1)[0] | used(k + 1)[1]
@@ -463,38 +487,34 @@
                     project_values(k + LEAD - 1, 1 - parity)
                 weigh(k, parity, h)
 
-        @pl.when(~needed)
-        def _():
-            if keying:
-                project_keys(k + LEAD, parity)
-            if valuing:
-                project_values(k + LEAD - 1, 1 - parity)
-
+        spare = [~needed & want for want in wants if want is not None]
         if keying:
-            share(0, k + LEAD, parity).start()
+            when(spare[0], lambda: project_keys(k + LEAD, parity))
         if valuing:
-            share(1, k + LEAD - 1, 1 - parity).start()
-
+            when(spare[-1], lambda: project_values(k + LEAD - 1, 1 - parity))
+        if keying:
+            when(wants[0], share(0, k + LEAD, parity).start)
+        if valuing:
+            when(wants[1], share(1, k + LEAD - 1, 1 - parity).start)
+
+    cross_pass(FAR)
+    for k in NEXT:
+        cross_start(k)
+    whole(3)
     share(0, 0, 0).wait_recv()
     for h in range(heads):
         score(0, 0, h, masked=True)
-    for k in NEXT:
-        cross_start(k)
-    whole(3)
+    prepare_keys(2)
+    prepare_values(2)
     prepare_keys(3)
-
-    def column(m, carry):
-        step(2 * m, 0)
-        step(2 * m + 1, 1)
-        return carry
-
-    lax.fori_loop(0, (count - LEAD) // 2, column, 0)
+    for k in range(count - LEAD):
+        step(k)
     for k in range(count - LEAD, count):
-        step(k, k % 2, scoring=k + 1 < count, keying=k + LEAD < count, valuing=k + LEAD - 1 < count)
+        step(k)
 
     for h in range(heads):
-        whole = acc[h]
-        att[:, h * VDIM : (h + 1) * VDIM] = (whole[:VDIM] / whole[VDIM : VDIM + 1]).T.astype(BF16)
+        summed = acc[h]
+        att[:, h * VDIM : (h + 1) * VDIM] = (summed[:VDIM] / summed[VDIM : VDIM + 1]).T.astype(BF16)
 
     ow_load.wait()
     width = ow.shape[1] // pieces
@@ -539,29 +559,29 @@
         side_out[late, j] = (kept[0, j] + pass_in[j].astype(F32)).astype(BF16)
         side_copy(late, j).start()
 
-    def out_copy(j):
-        part = pl.ds(j * width, width)
-        return pltpu.make_async_copy(out.at[:, part], out_hbm.at[:, part], out_sem.at[0])
-
     for j in order:
         side_copy(0, j).wait_recv()
         side_copy(1, j).wait_recv()
         total = kept[1, j] + side_in[0, j].astype(F32) + side_in[1, j].astype(F32)
-        out[:, j * width : (j + 1) * width] = total.astype(BF16)
-        out_copy(j).start()
+        out_ref[:, j * width : (j + 1) * width] = total.astype(BF16)
 
     def all_sent(ref, send_sem):
         send(ref, beside, send_sem.at[0], send_sem.at[0]).wait_send()
 
     all_sent(kv.at[pl.ds(0, SENT * rows)], kv_send)
-    for n, refs in enumerate((own_keys, own_values)):
-        for ref in refs:
-            send(ref, beside, share_send.at[n], share_send.at[n]).wait_send()
+    for n, (into, always) in enumerate(((keys_in, LEAD), (values_in, LEAD - 1))):
+        shared = always
+        for k in range(always, count):
+            shared = shared + jnp.where(needs(k)[0], 1, 0)
+        for k in range(always, count + 1):
+            pl.when(shared == k)(send(into.at[pl.ds(0, k)], beside, share_send.at[n], share_send.at[n]).wait_send)
+    for k in range(LEAD, count):
+        if is_late(k):
+            pl.when(~needs(k)[0])(lambda k=k: finish(k))
     all_sent(kv.at[pl.ds(0, 3 * rows)], line_send)
     all_sent(ql.at[pl.ds(0, 3 * rows)], q_send)
     all_sent(side_out, side_send)
     all_sent(pass_out, pass_send)
-    pltpu.make_async_copy(out, out_hbm, out_sem.at[0]).wait()
 
 
 def solution(mesh):
@@ -586,9 +606,9 @@
         like = lambda a: pltpu.VMEM(a.shape, a.dtype)
         total = pl.pallas_call(
             functools.partial(kernel, S, T, chunks, pieces),
-            out_shape=jax.ShapeDtypeStruct((rows, width), BF16),
+            out_shape=pltpu.VMEM((rows, width), BF16),
             in_specs=[hbm] * 13,
-            out_specs=hbm,
+            out_specs=pl.BlockSpec(memory_space=pltpu.VMEM),
             scratch_shapes=[
                 like(tokens),
                 like(dq),
@@ -623,13 +643,11 @@
                 pltpu.VMEM((heads, 8, span), F32),
                 pltpu.VMEM((span, LANES), F32),
                 pltpu.VMEM((span, LANES), F32),
-                pltpu.VMEM((rows, width), BF16),
                 pltpu.VMEM((1, dq.shape[1]), F32),
                 pltpu.VMEM((1, rank), F32),
                 pltpu.VMEM(tables[0].shape, F32),
                 pltpu.VMEM(tables[1].shape, F32),
                 dma(2 * chunks + 13),
-                dma(1),
                 dma(1),
                 dma(4),
                 dma(1),

time: 63.9 us -> 61 us (0.955)
  Pallas kernels: 61.7 us -> 60.1 us
  local copies, waits for them, and re-layouts: 1.87 us -> 0.8 us
    pallas_call x1, Pallas kernels: 61.7 us -> 60.1 us  [local(): pl.pallas_call(functools.partial(kernel, S, T, chunks, pieces), out_shape...]
    unnamed x1, local copies, waits for them, and re-layouts: 1.87 us -> 0.8 us
where the time goes in v5:
time: 61 us; the launch traced here: 60.9 us
  Pallas kernels  60.1 us (99%)
  local copies, waits for them, and re-layouts  0.8 us (1%)
    pallas_call x1, Pallas kernels, local(): pl.pallas_call(functools.partial(kernel, S, T, chunks, pieces), out_shape...  60.1 us

profile of v5, /device:TPU:65, one launch (start us, length us, event | category | flops | bytes accessed | tf_op | source)
XLA Modules:
  0.0 60.9 jit_solution(8357120362194495865)
XLA Ops:
  0.0 60.1 %shard_map.127 = bf16[64,4096]{1,0:T(8,128)(2,1)S(1)} custom-call(bf16[64,4096]{1,0:T(8,128)(2,1)} %tokens_hbm.1, bf16[4096,1024]{1,0:T(8,128)(2,1)} %dq_hbm.1, bf16[4096,512]{1,0:T(8,128)(2,1)} %dl_hbm.1, bf16[64,4096]{1,0:T(8,128)(2,1)} %bitcast.3, f32[1,1024]{1,0:T(1,128)} %bitcast.4, f32[1,512]{1,0:T(1,128)} %bitcast.5, bf16[1024,512]{1,0:T(8,128)(2,1)} %uq_hbm.1, ...), custom_call_target="tpu_custom_call" | custom-call | tf_op jit(solution)/shard_map/pallas_call | solution.py:607
  60.1 0.8 %copy.15 = bf16[64,4096]{1,0:T(8,128)(2,1)} copy(bf16[64,4096]{1,0:T(8,128)(2,1)S(1)} %shard_map.127) | data formatting | bytes 1048576

commit v6 on v5

--- a/solution.py
+++ b/solution.py
@@ -388,8 +388,13 @@
     prepare_values(1)
     for n in range(2):
         q_line[3](n)
+    cross_pass(FAR)
+    for k in NEXT:
+        cross_start(k)
+    whole(3)
     for copy in up_loads[:2]:
         copy.wait()
+    share(0, 0, 0).wait_recv()
     scale = (NOPE + ROPE) ** (-0.5) * log2e
     plain = (dot(ql[...], uq[...]) * scale).astype(BF16)
     turning = dot(ql[...], ur[...]) * scale
@@ -402,6 +407,9 @@
         qh[h, :, :NOPE] = plain[:, h * NOPE : (h + 1) * NOPE]
         best[h] = jnp.full(best.shape[1:], masked_score, F32)
         acc[h] = jnp.zeros(acc.shape[1:], F32)
+    project_keys(2, 0)
+    project_values(2, 0)
+    project_keys(3, 1)
 
     def used(k):
         return (sp >= 0, i == 1) if k == 0 else needs(k)
@@ -479,13 +487,13 @@
         @pl.when(needed)
         def _():
             for h in range(heads):
-                if scoring:
-                    score(k + 1, 1 - parity, h)
+                weigh(k, parity, h)
                 if keying and h == 0:
                     project_keys(k + LEAD, parity)
                 if valuing and h == 2:
                     project_values(k + LEAD - 1, 1 - parity)
-                weigh(k, parity, h)
+                if scoring:
+                    score(k + 1, 1 - parity, h)
 
         spare = [~needed & want for want in wants if want is not None]
         if keying:
@@ -497,16 +505,10 @@
         if valuing:
             when(wants[1], share(1, k + LEAD - 1, 1 - parity).start)
 
-    cross_pass(FAR)
-    for k in NEXT:
-        cross_start(k)
-    whole(3)
-    share(0, 0, 0).wait_recv()
     for h in range(heads):
         score(0, 0, h, masked=True)
-    prepare_keys(2)
-    prepare_values(2)
-    prepare_keys(3)
+    for copy in (share(0, 2, 0), share(1, 2, 0), share(0, 3, 1)):
+        copy.start()
     for k in range(count - LEAD):
         step(k)
     for k in range(count - LEAD, count):
@@ -535,9 +537,8 @@
         return exchange(pass_out.at[j], pass_in.at[j], target, pass_send.at[0], pass_recv.at[j])
 
     def side_copy(side, j):
-        n = side * pieces + j
         target = (right, left)[side]
-        return exchange(side_out.at[side, j], side_in.at[side, j], target, side_send.at[0], side_recv.at[n])
+        return exchange(side_out.at[side, j], side_in.at[j, side], target, side_send.at[0], side_recv.at[j])
 
     attended = jnp.concatenate([att[block_rows(t), :] for t in (opposite, right, left, tp)], axis=0)
     for n in range(pieces):
@@ -560,9 +561,8 @@
         side_copy(late, j).start()
 
     for j in order:
-        side_copy(0, j).wait_recv()
-        side_copy(1, j).wait_recv()
-        total = kept[1, j] + side_in[0, j].astype(F32) + side_in[1, j].astype(F32)
+        exchange(side_in.at[j], side_in.at[j], left, side_send.at[0], side_recv.at[j]).wait_recv()
+        total = kept[1, j] + side_in[j, 0].astype(F32) + side_in[j, 1].astype(F32)
         out_ref[:, j * width : (j + 1) * width] = total.astype(BF16)
 
     def all_sent(ref, send_sem):
@@ -626,7 +626,7 @@
                 pltpu.VMEM((heads, 8, span), F32),
                 pltpu.VMEM((span, heads * VDIM), BF16),
                 pltpu.VMEM((2, pieces, rows, width // pieces), BF16),
-                pltpu.VMEM((2, pieces, rows, width // pieces), BF16),
+                pltpu.VMEM((pieces, 2, rows, width // pieces), BF16),
                 pltpu.VMEM((2, pieces, rows, width // pieces), F32),
                 pltpu.VMEM((pieces, rows, width // pieces), BF16),
                 pltpu.VMEM((pieces, rows, width // pieces), BF16),
@@ -657,7 +657,7 @@
                 dma(1),
                 dma(4),
                 dma(1),
-                dma(2 * pieces),
+                dma(pieces),
                 dma(1),
                 dma(pieces),
             ],

time: 61 us -> 60.8 us (level)
  no operation moved by 1% of the time
where the time goes in v6:
time: 60.8 us; the launch traced here: 60.7 us
  Pallas kernels  59.9 us (99%)
  local copies, waits for them, and re-layouts  0.8 us (1%)
    pallas_call x1, Pallas kernels, local(): pl.pallas_call(functools.partial(kernel, S, T, chunks, pieces), out_shape...  59.9 us

profile of v6, /device:TPU:65, one launch (start us, length us, event | category | flops | bytes accessed | tf_op | source)
XLA Modules:
  0.0 60.7 jit_solution(11160784900105817402)
XLA Ops:
  0.0 59.9 %shard_map.127 = bf16[64,4096]{1,0:T(8,128)(2,1)S(1)} custom-call(bf16[64,4096]{1,0:T(8,128)(2,1)} %tokens_hbm.1, bf16[4096,1024]{1,0:T(8,128)(2,1)} %dq_hbm.1, bf16[4096,512]{1,0:T(8,128)(2,1)} %dl_hbm.1, bf16[64,4096]{1,0:T(8,128)(2,1)} %bitcast.3, f32[1,1024]{1,0:T(1,128)} %bitcast.4, f32[1,512]{1,0:T(1,128)} %bitcast.5, bf16[1024,512]{1,0:T(8,128)(2,1)} %uq_hbm.1, ...), custom_call_target="tpu_custom_call" | custom-call | tf_op jit(solution)/shard_map/pallas_call | solution.py:607
  59.9 0.8 %copy.15 = bf16[64,4096]{1,0:T(8,128)(2,1)} copy(bf16[64,4096]{1,0:T(8,128)(2,1)S(1)} %shard_map.127) | data formatting | bytes 1048576
